TPU v7x, 32 devices: a whole 2x2x4 slice. The times are simulated.
32 devices in a mesh: sp: 16 (over z, y, x), tp: 2 (over core).
Axes of the slice: x: 2, y: 2, z: 4, core: 2. Of those that a mesh axis runs over, the one named last changes fastest.
Arguments:
- stream: bfloat16 [6144, 2048], P('sp'), may hold values from -40 to 40
- query_rows: bfloat16 [6144, 1024], P('sp', 'tp'), may hold values from -10 to 10
- key_rows: bfloat16 [6144, 256], P('sp'), may hold values from -10 to 10
- value_rows: bfloat16 [6144, 256], P('sp'), may hold values from -6 to 6
- doc_ids: int32 [6144], P('sp'), may hold values from 0 to 7, never falling along the last dimension, each value on 1 to 1536 neighbouring positions
- sink_logit: float32 [8], P('tp'), may hold values from 2 to 7
- out_weight: bfloat16 [1024, 2048], P('tp'), may hold values from -1.5 to 1.5
- norm_gain: float32 [2048], replicated, may hold values from 0.1 to 1.9
- gate_weight: bfloat16 [2048, 5632], P('sp', 'tp'), may hold values from -0.125 to 0.125
- up_weight: bfloat16 [2048, 5632], P('sp', 'tp'), may hold values from -0.125 to 0.125
- down_weight: bfloat16 [5632, 2048], P('tp', 'sp'), may hold values from -0.078125 to 0.078125
Outputs:
- mixed_out: bfloat16 [6144, 2048], P('sp')
Inputs may be any that keep to these rules, and one draw needn't show every extreme that they name: `doc_ids`: document numbers never fall along the sequence; each document has 1 to 1536 positions.
All inputs are finite; a program needn't handle non-finite values.
Results may differ from a plain program's by a relative error of at most 0.009.
Values may be sent and summed in bfloat16 or wider, within the bound.
A program may use at most 128 MiB of HBM per device.

v0:
```python
import jax
import jax.numpy as jnp
from jax import lax
from jax.sharding import Mesh, PartitionSpec as P

HEADS = 8
KVH = 2
HD = 128
WIN = 128

norm_eps = 1e-06
masked_low = -1e30
SP = ("sa", "sb")


def halo(value, width):
    peers = lax.axis_size(SP)
    length = value.shape[0]
    up = [(i, i + 1) for i in range(peers - 1)]
    down = [(j, i) for i, j in up]
    before = lax.ppermute(value[length - width :], SP, up)
    after = lax.ppermute(value[:width], SP, down)
    return jnp.concatenate([before, value, after], axis=0)


def exchange(blocks):
    peers = lax.axis_size("sa")
    here = lax.axis_index("sa")
    got = [lax.dynamic_index_in_dim(blocks, here, 0, keepdims=True)]
    for k in range(1, peers):
        out = lax.dynamic_index_in_dim(blocks, lax.rem(here + k, peers), 0, keepdims=True)
        got.append(lax.ppermute(out, "sa", [(i, (i + k) % peers) for i in range(peers)]))
    ring = got[::-1]
    both = jnp.concatenate(ring + ring, axis=0)
    return lax.dynamic_slice_in_dim(both, peers - 1 - here, peers, 0)


def per_device(
    stream,
    query_rows,
    key_rows,
    value_rows,
    doc_ids,
    sink_logit,
    out_weight,
    norm_gain,
    gate_weight,
    up_weight,
    down_weight,
):
    row_count, width = stream.shape
    n_a, n_b, n_tp = lax.axis_size("sa"), lax.axis_size("sb"), lax.axis_size("tp")
    depth, hidden_here = gate_weight.shape
    share = hidden_here // n_a
    tp_place = lax.axis_index("tp")
    sp_place = lax.axis_index(SP)

    def shares(w):
        return w.reshape(depth, n_a, share).transpose(1, 0, 2)

    gate_up = exchange(jnp.concatenate([shares(gate_weight), shares(up_weight)], axis=2))
    gate_up = gate_up.reshape(n_a * depth, 2 * share)
    gate_up = lax.all_gather(gate_up, "sb", axis=0, tiled=True)
    down_mine = exchange(down_weight.reshape(n_a, share, depth))
    down_mine = down_mine.transpose(0, 2, 1).reshape(n_a * depth, share)

    heads_here = query_rows.shape[1] // HD
    group_share = HEADS // KVH
    groups_here = max(1, heads_here // group_share)
    per_group = heads_here // groups_here
    group_first = tp_place * heads_here // group_share
    keys_here = lax.dynamic_slice_in_dim(key_rows, group_first * HD, groups_here * HD, 1)
    values_here = lax.dynamic_slice_in_dim(value_rows, group_first * HD, groups_here * HD, 1)
    docs_col = jnp.broadcast_to(doc_ids.astype(jnp.bfloat16)[:, None], (row_count, HD))
    packed = halo(jnp.concatenate([keys_here, values_here, docs_col], axis=1), WIN)
    span = groups_here * HD
    keys_wide, values_wide = packed[:, :span], packed[:, span : 2 * span]
    docs_wide = packed[:, 2 * span].astype(jnp.int32)
    seq_offset = sp_place * row_count
    seq_total = row_count * n_a * n_b
    query_pos = seq_offset + jnp.arange(row_count, dtype=jnp.int32)
    key_pos = seq_offset - WIN + jnp.arange(row_count + 2 * WIN, dtype=jnp.int32)
    allowed = (
        (jnp.abs(query_pos[:, None] - key_pos[None, :]) <= WIN)
        & (key_pos[None, :] >= 0)
        & (key_pos[None, :] < seq_total)
        & (doc_ids[:, None] == docs_wide[None, :])
    )
    queries = query_rows.reshape(row_count, groups_here, per_group, HD)
    keys_grid = keys_wide.reshape(row_count + 2 * WIN, groups_here, HD)
    values_grid = values_wide.reshape(row_count + 2 * WIN, groups_here, HD)
    scores = jnp.einsum(
        "qgrd,kgd->grqk", queries, keys_grid, preferred_element_type=jnp.float32
    ) * HD ** (-0.5)
    masked = jnp.where(allowed[None, None], scores, masked_low)
    sinks = sink_logit.reshape(groups_here, per_group, 1, 1)
    peak = jnp.maximum(jnp.max(masked, axis=-1, keepdims=True), sinks)
    lifted = jnp.where(allowed[None, None], jnp.exp(masked - peak), 0.0)
    denom = jnp.sum(lifted, axis=-1, keepdims=True) + jnp.exp(sinks - peak)
    probs = (lifted / denom).astype(jnp.bfloat16)
    attended = jnp.einsum("grqk,kgd->qgrd", probs, values_grid, preferred_element_type=jnp.float32)
    attended = attended.astype(jnp.bfloat16).reshape(row_count, heads_here * HD)
    partial_value = jnp.dot(attended, out_weight, preferred_element_type=jnp.float32)

    rows_mine = row_count // n_tp
    branch = lax.psum_scatter(
        partial_value.astype(jnp.bfloat16), "tp", scatter_dimension=0, tiled=True
    )
    stream_mine = lax.dynamic_slice_in_dim(stream, tp_place * rows_mine, rows_mine, 0)
    carried = (stream_mine.astype(jnp.float32) + branch.astype(jnp.float32)).astype(jnp.bfloat16)
    carried_f = carried.astype(jnp.float32)
    normed = (
        carried_f
        * lax.rsqrt(jnp.mean(carried_f * carried_f, axis=1, keepdims=True) + norm_eps)
        * norm_gain[None, :]
    ).astype(jnp.bfloat16)
    normed = normed.reshape(rows_mine, n_a, n_b, depth).transpose(0, 2, 1, 3).reshape(rows_mine, width)
    rows_all = lax.all_gather(normed, ("sa", "tp"), axis=0, tiled=True)
    down_mine, _ = lax.optimization_barrier((down_mine, normed))
    down_all = lax.all_gather(down_mine, "sb", axis=0, tiled=True)

    gate_acc = jnp.dot(rows_all, gate_up[:, :share], preferred_element_type=jnp.float32)
    up_acc = jnp.dot(rows_all, gate_up[:, share:], preferred_element_type=jnp.float32)
    hidden = (jax.nn.silu(gate_acc) * up_acc).astype(jnp.bfloat16)
    terms = lax.dot_general(
        hidden, down_all, (((1,), (1,)), ((), ())), preferred_element_type=jnp.float32
    )
    feed = lax.psum_scatter(
        terms.astype(jnp.bfloat16), ("sa", "tp"), scatter_dimension=0, tiled=True
    )
    feed = feed.reshape(rows_mine, n_b, n_a, depth).transpose(0, 2, 1, 3).reshape(rows_mine, width)
    mixed = (carried_f + 0.5 * feed.astype(jnp.float32)).astype(jnp.bfloat16)
    return lax.all_gather(mixed, "tp", axis=0, tiled=True)


def solution(mesh):
    n_sp, n_tp = mesh.shape["sp"], mesh.shape["tp"]
    n_a = 4 if n_sp % 4 == 0 else 1
    fine = Mesh(mesh.devices.reshape(n_a, n_sp // n_a, n_tp), ("sa", "sb", "tp"))
    in_specs = (
        P(SP, None),
        P(SP, "tp"),
        P(SP, None),
        P(SP, None),
        P(SP),
        P("tp"),
        P("tp", None),
        P(),
        P(SP, "tp"),
        P(SP, "tp"),
        P("tp", SP),
    )
    return jax.shard_map(
        per_device, mesh=fine, in_specs=in_specs, out_specs=P(SP, None), check_vma=False
    )
```

profile of v0, /device:TPU:0, one launch (start us, length us, event | category | flops | bytes accessed | tf_op | source)
XLA Modules:
  0.0 361.3 jit_solution(14193642974242643932)
XLA Ops:
  9.3 4.9 %collective-permute-start = (bf16[128,384]{1,0:T(8,128)(2,1)S(1)}, bf16[128,384]{1,0:T(8,128)(2,1)S(1)}, u32[]{:S(2)}, u32[]{:S(2)}) collective-permute-start(bf16[128,384]{1,0:T(8,128)(2,1)S(1)} %get-tuple-element.16), channel_id=1, source_target_pairs={{0,2},{2,4},{4,6},{6,8},{8,10},{10,12},{12,14},{14,16},{16,18},{18... | collective-permute-start | bytes 294920 | tf_op jit(solution)/shard_map/ppermute | solution.py:21
  14.2 1.3 collective-permute-start.1
  16.4 4.3 %collective-permute-done.1 = bf16[128,384]{1,0:T(8,128)(2,1)S(1)} collective-permute-done((bf16[128,384]{1,0:T(8,128)(2,1)S(1)}, bf16[128,384]{1,0:T(8,128)(2,1)S(1)}, u32[]{:S(2)}, u32[]{:S(2)}) %collective-permute-start.1) | collective-permute-done | bytes 98336 | tf_op jit(solution)/shard_map/ppermute | solution.py:22
  21.0 1.4 fusion.16
  22.4 1.8 fusion
  25.3 1.5 fusion.11
  26.9 2.2 convolution_convert_fusion.1
  30.7 3.6 collective-permute-start.2
  35.3 8.2 %collective-permute-done.2 = bf16[1,128,1408]{1,2,0:T(8,128)(2,1)S(1)} collective-permute-done((bf16[1,128,1408]{1,2,0:T(8,128)(2,1)}, bf16[1,128,1408]{1,2,0:T(8,128)(2,1)S(1)}, u32[]{:S(2)}, u32[]{:S(2)}) %collective-permute-start.2) | collective-permute-done | bytes 360480 | tf_op jit(solution)/shard_map/ppermute | solution.py:32
  43.5 20.6 %collective-permute-done.3 = bf16[1,128,1408]{1,2,0:T(8,128)(2,1)S(1)} collective-permute-done((bf16[1,128,1408]{1,2,0:T(8,128)(2,1)S(1)}, bf16[1,128,1408]{1,2,0:T(8,128)(2,1)S(1)}, u32[]{:S(2)}, u32[]{:S(2)}) %collective-permute-start.3) | collective-permute-done | bytes 360480 | tf_op jit(solution)/shard_map/ppermute | solution.py:32
  64.6 1.6 copy.22
  66.2 1.7 fusion.7
  69.2 1.5 reshape.242
  70.8 1.2 constant_dynamic-slice_fusion.1
  72.7 2.6 collective-permute-start.6
  75.5 2.1 collective-permute-start.7
  77.9 3.3 collective-permute-done.5
  81.2 24.5 %collective-permute-done.6 = bf16[1,704,128]{2,0,1:T(2,128)(2,1)S(1)} collective-permute-done((bf16[1,704,128]{2,0,1:T(2,128)(2,1)S(1)}, bf16[1,704,128]{2,0,1:T(2,128)(2,1)S(1)}, u32[]{:S(2)}, u32[]{:S(2)}) %collective-permute-start.6) | collective-permute-done | bytes 180256 | tf_op jit(solution)/shard_map/ppermute | solution.py:32
  106.5 7.4 %concatenate.19 = bf16[8,704,128]{2,0,1:T(8,128)(2,1)S(1)} concatenate(bf16[1,704,128]{2,0,1:T(2,128)(2,1)S(1)} %collective-permute-done.5, bf16[1,704,128]{2,0,1:T(2,128)(2,1)} %copy-done.2, bf16[1,704,128]{2,0,1:T(2,128)(2,1)} %collective-permute-done.7, bf16[1,704,128]{2,0,1:T(2,128)(2,1)S(1)} %copy.34, bf16[1,704,128]{2,0,1:T(2,128)(2,1)S(1)} %collective-permute-done.5, ...), dimensions={0} | concatenate | bytes 2883584 | tf_op jit(solution)/shard_map/concatenate | solution.py:34
  115.5 16.2 %all-gather.7.cloned.1.call-done = bf16[2048,1408]{1,0:T(8,128)(2,1)} async-done(((bf16[512,1408]{1,0:T(8,128)(2,1)}), bf16[2048,1408]{1,0:T(8,128)(2,1)}) %all-gather.7.cloned.1.call-update) | async-done | bytes 5767184 | tf_op jit(solution)/shard_map/all_gather | solution.py:63
  131.7 66.1 %all-gather.5.cloned.1.call-done = bf16[1536,2048]{1,0:T(8,128)(2,1)} async-done(((bf16[192,2048]{1,0:T(8,128)(2,1)}), bf16[1536,2048]{1,0:T(8,128)(2,1)}) %all-gather.5.cloned.1.call-update) | async-done | bytes 6291472 | tf_op jit(solution)/shard_map/all_gather | solution.py:118
  197.8 10.5 %fusion.2 = f32[1536,704]{0,1:T(8,128)} fusion(bf16[1536,2048]{1,0:T(8,128)(2,1)} %all-gather.5.cloned.1.call-done, bf16[2048,1408]{1,0:T(8,128)(2,1)} %all-gather.7.cloned.1.call-done), kind=kOutput, calls=%fused_computation.7 | convolution fusion | flops 4429185024 | bytes 13762560 | tf_op jit(solution)/shard_map/dot_general | solution.py:122
  208.3 31.3 %all-gather.9.cloned.1.call-done = bf16[2048,704]{0,1:T(8,128)(2,1)} async-done(((bf16[512,704]{0,1:T(8,128)(2,1)}), bf16[2048,704]{0,1:T(8,128)(2,1)}) %all-gather.9.cloned.1.call-update) | async-done | bytes 2883600 | tf_op jit(solution)/shard_map/all_gather | solution.py:120
  239.6 21.3 %convolution_convert_fusion = bf16[1536,2048]{1,0:T(8,128)(2,1)} fusion(bf16[2048,704]{0,1:T(8,128)(2,1)} %all-gather.9.cloned.1.call-done, f32[1536,704]{0,1:T(8,128)} %fusion.2, bf16[1536,2048]{1,0:T(8,128)(2,1)} %all-gather.5.cloned.1.call-done, bf16[2048,1408]{1,0:T(8,128)(2,1)} %all-gather.7.cloned.1.call-done), kind=kOutput, calls=%fused_computation | convolution fusion | flops 8868003840 | bytes 22937600 | tf_op jit(solution)/shard_map/dot_general | solution.py:125
  261.1 69.4 %reduce-scatter.5.cloned.1.call-done = bf16[192,2048]{1,0:T(8,128)(2,1)} async-done(((bf16[1536,2048]{1,0:T(8,128)(2,1)}), bf16[192,2048]{1,0:T(8,128)(2,1)}) %reduce-scatter.5.cloned.1.call-update) | async-done | bytes 786448 | tf_op jit(solution)/shard_map/reduce_scatter | solution.py:128
  330.6 1.3 convert_multiply_fusion.2
  331.9 2.2 mul.87
  334.1 3.0 copy.46
  337.1 2.9 mul.89
  340.0 2.5 fusion.10
  342.5 8.5 %all-gather.11.cloned.1.call-done = bf16[384,2048]{1,0:T(8,128)(2,1)} async-done(((bf16[192,2048]{1,0:T(8,128)(2,1)}), bf16[384,2048]{1,0:T(8,128)(2,1)}) %all-gather.11.cloned.1.call-update) | async-done | bytes 1572880 | tf_op jit(solution)/shard_map/all_gather | solution.py:133
  351.0 2.7 copy.57
  (67 shorter events, 12.5 us)
Async XLA Ops:
  7.4 19.5 %copy-start = (bf16[512,2048]{1,0:T(8,128)(2,1)S(1)}, bf16[512,2048]{1,0:T(8,128)(2,1)}, u32[]{:S(2)}) copy-start(bf16[512,2048]{1,0:T(8,128)(2,1)} %param.17) | copy-start | bytes 6291460
  7.4 58.9 %reduce-scatter.3.cloned.1.call-start = ((), (), s32[]{:S(2)}) async-start(), calls=%async_computation.2 | async-start | bytes 2359296 | tf_op jit(solution)/shard_map/reduce_scatter | solution.py:106
  9.3 7.1 %collective-permute-start = (bf16[128,384]{1,0:T(8,128)(2,1)S(1)}, bf16[128,384]{1,0:T(8,128)(2,1)S(1)}, u32[]{:S(2)}, u32[]{:S(2)}) collective-permute-start(bf16[128,384]{1,0:T(8,128)(2,1)S(1)} %get-tuple-element.16), channel_id=1, source_target_pairs={{0,2},{2,4},{4,6},{6,8},{8,10},{10,12},{12,14},{14,16},{16,18},{18... | collective-permute-start | bytes 294920 | tf_op jit(solution)/shard_map/ppermute | solution.py:21
  14.2 6.5 %collective-permute-start.1 = (bf16[128,384]{1,0:T(8,128)(2,1)S(1)}, bf16[128,384]{1,0:T(8,128)(2,1)S(1)}, u32[]{:S(2)}, u32[]{:S(2)}) collective-permute-start(bf16[128,384]{1,0:T(8,128)(2,1)S(1)} %get-tuple-element.17), channel_id=1, source_target_pairs={{2,0},{4,2},{6,4},{8,6},{10,8},{12,10},{14,12},{16,14},{18,16},{20... | collective-permute-start | bytes 294920 | tf_op jit(solution)/shard_map/ppermute | solution.py:22
  15.6 8.7 %copy-start.6 = (f32[4]{0:T(128)S(1)}, f32[4]{0:T(128)}, u32[]{:S(2)}) copy-start(f32[4]{0:T(128)} %param.16) | copy-start | bytes 52
  26.8 2.3 copy-start.3
  26.8 2.6 copy-start.4
  29.0 102.7 %all-gather.7.cloned.1.call-start = ((), (), s32[]{:S(2)}) async-start(), calls=%async_computation.4 | async-start | bytes 7208960 | tf_op jit(solution)/shard_map/all_gather | solution.py:63
  30.7 12.8 %collective-permute-start.2 = (bf16[1,128,1408]{1,2,0:T(8,128)(2,1)}, bf16[1,128,1408]{1,2,0:T(8,128)(2,1)S(1)}, u32[]{:S(2)}, u32[]{:S(2)}) collective-permute-start(bf16[1,128,1408]{1,2,0:T(8,128)(2,1)} %get-tuple-element.10), channel_id=1, source_target_pairs={{0,24},{8,0},{16,8},{24,16},{1,25},{9,1},{17,9},{25,17},{2,26},{10... | collective-permute-start | bytes 1081352 | tf_op jit(solution)/shard_map/ppermute | solution.py:32
  34.3 29.7 %collective-permute-start.3 = (bf16[1,128,1408]{1,2,0:T(8,128)(2,1)S(1)}, bf16[1,128,1408]{1,2,0:T(8,128)(2,1)S(1)}, u32[]{:S(2)}, u32[]{:S(2)}) collective-permute-start(bf16[1,128,1408]{1,2,0:T(8,128)(2,1)S(1)} %get-tuple-element.11), channel_id=1, source_target_pairs={{0,16},{8,24},{16,0},{24,8},{1,17},{9,25},{17,1},{25,9},{2,18},{10... | collective-permute-start | bytes 1081352 | tf_op jit(solution)/shard_map/ppermute | solution.py:32
  34.3 29.8 %collective-permute-start.4 = (bf16[1,128,1408]{1,2,0:T(8,128)(2,1)S(1)}, bf16[1,128,1408]{1,2,0:T(8,128)(2,1)S(1)}, u32[]{:S(2)}, u32[]{:S(2)}) collective-permute-start(bf16[1,128,1408]{1,2,0:T(8,128)(2,1)S(1)} %get-tuple-element.9), channel_id=1, source_target_pairs={{0,8},{8,16},{16,24},{24,0},{1,9},{9,17},{17,25},{25,1},{2,10},{10... | collective-permute-start | bytes 1081352 | tf_op jit(solution)/shard_map/ppermute | solution.py:32
  64.6 3.4 copy-start.5
  66.2 131.6 %all-gather.5.cloned.1.call-start = ((), (), s32[]{:S(2)}) async-start(), calls=%async_computation.3 | async-start | bytes 7077888 | tf_op jit(solution)/shard_map/all_gather | solution.py:118
  70.7 168.9 %all-gather.9.cloned.1.call-start = ((), (), s32[]{:S(2)}) async-start(), calls=%async_computation.5 | async-start | bytes 3604480 | tf_op jit(solution)/shard_map/all_gather | solution.py:120
  72.3 8.9 %collective-permute-start.5 = (bf16[1,704,128]{2,0,1:T(2,128)(2,1)S(1)}, bf16[1,704,128]{2,0,1:T(2,128)(2,1)S(1)}, u32[]{:S(2)}, u32[]{:S(2)}) collective-permute-start(bf16[1,704,128]{2,0,1:T(2,128)(2,1)S(1)} %copy.31), channel_id=1, source_target_pairs={{0,24},{8,0},{16,8},{24,16},{1,25},{9,1},{17,9},{25,17},{2,26},{10... | collective-permute-start | bytes 540680 | tf_op jit(solution)/shard_map/ppermute | solution.py:32
  72.7 33.0 %collective-permute-start.6 = (bf16[1,704,128]{2,0,1:T(2,128)(2,1)S(1)}, bf16[1,704,128]{2,0,1:T(2,128)(2,1)S(1)}, u32[]{:S(2)}, u32[]{:S(2)}) collective-permute-start(bf16[1,704,128]{2,0,1:T(2,128)(2,1)S(1)} %copy.32), channel_id=1, source_target_pairs={{0,16},{8,24},{16,0},{24,8},{1,17},{9,25},{17,1},{25,9},{2,18},{10... | collective-permute-start | bytes 540680 | tf_op jit(solution)/shard_map/ppermute | solution.py:32
  75.5 30.9 %collective-permute-start.7 = (bf16[1,704,128]{2,0,1:T(2,128)(2,1)S(1)}, bf16[1,704,128]{2,0,1:T(2,128)(2,1)}, u32[]{:S(2)}, u32[]{:S(2)}) collective-permute-start(bf16[1,704,128]{2,0,1:T(2,128)(2,1)S(1)} %copy.33), channel_id=1, source_target_pairs={{0,8},{8,16},{16,24},{24,0},{1,9},{9,17},{17,25},{25,1},{2,10},{10... | collective-permute-start | bytes 540680 | tf_op jit(solution)/shard_map/ppermute | solution.py:32
  105.7 0.7 copy-start.2
  115.3 215.3 %reduce-scatter.5.cloned.1.call-start = ((), (), s32[]{:S(2)}) async-start(), calls=%async_computation.6 | async-start | bytes 7077888 | tf_op jit(solution)/shard_map/reduce_scatter | solution.py:128
  260.9 90.1 %all-gather.11.cloned.1.call-start = ((), (), s32[]{:S(2)}) async-start(), calls=%async_computation.7 | async-start | bytes 2359296 | tf_op jit(solution)/shard_map/all_gather | solution.py:133
  337.1 16.7 %copy-start.1 = (bf16[512,2048]{1,0:T(8,128)(2,1)S(1)}, bf16[512,2048]{1,0:T(8,128)(2,1)}, u32[]{:S(2)}) copy-start(bf16[512,2048]{1,0:T(8,128)(2,1)} %param.17) | copy-start | bytes 6291460
Sparse Core Ops, SparseCore 0:
  29.2 11.0 reduce-scatter.2
  342.6 8.3 all-gather.10
Sparse Core Ops, SparseCore 1:
  66.2 65.4 all-gather.6
  133.2 64.5 all-gather.4
  199.5 40.0 all-gather.8
  260.9 69.6 reduce-scatter.4
where the time goes:
time: 362 us; the launch traced here: 361 us
  waiting for transfers between devices  253 us (70%)
  matrix products  37.1 us (10%)
  local copies, waits for them, and re-layouts  28.9 us (8%)
  starting transfers between devices  16.1 us (4%)
  between operations  15.4 us (4%)
  other arithmetic  10.4 us (3%)
    reduce_scatter x1, waiting for transfers between devices, per_device(): lax.psum_scatter(terms.astype(jnp.bfloat16), ('sa', 'tp'), scatter_dimens...  69.4 us
    all_gather x1, waiting for transfers between devices, per_device(): rows_all = lax.all_gather(normed, ('sa', 'tp'), axis=0, tiled=True)  66.1 us
    ppermute x6, waiting for transfers between devices, exchange(): lax.ppermute(out, 'sa', [(i, (i + k) % peers) for i in range(peers)])  56.5 us
    all_gather x1, waiting for transfers between devices, per_device(): down_all = lax.all_gather(down_mine, 'sb', axis=0, tiled=True)  31.3 us
    dot_general x1, matrix products, per_device(): lax.dot_general(hidden, down_all, (((1,), (1,)), ((), ())), preferred_ele...  21.3 us
    all_gather x1, waiting for transfers between devices, per_device(): gate_up = lax.all_gather(gate_up, 'sb', axis=0, tiled=True)  16.2 us
    dot_general x1, matrix products, per_device(): jnp.dot(rows_all, gate_up[:, :share], preferred_element_type=jnp.float32)  10.5 us
    ppermute x6, starting transfers between devices, exchange(): lax.ppermute(out, 'sa', [(i, (i + k) % peers) for i in range(peers)])  9.32 us
  transfers between devices with their start and end apart: 14, of which 11 were waited for; matrix products, arithmetic and copies ran while one was open for 8% of the time, Pallas kernels for 0%

commit v1 on v0

--- a/solution.py
+++ b/solution.py
@@ -1,6 +1,8 @@
 import jax
 import jax.numpy as jnp
 from jax import lax
+from jax.experimental import pallas as pl
+from jax.experimental.pallas import tpu as pltpu
 from jax.sharding import Mesh, PartitionSpec as P
 
 HEADS = 8
@@ -133,23 +135,456 @@
     return lax.all_gather(mixed, "tp", axis=0, tiled=True)
 
 
+MESH = pl.DeviceIdType.MESH
+AX = ("sa", "sy", "sx", "tp")
+
+
+def fused(
+    stream_ref, query_ref, key_ref, value_ref, docs_ref, sink_ref, out_w_ref, gain_ref, own_w_ref,
+    mixed_ref,
+    keys, values, docs, attended, branch_out, branch_in, carried_keep, rows, weights, hidden_keep,
+    sum_keep, pair_out, pair_in, chain_out, chain_fwd, chain_back,
+    halo_s, halo_r, a2a_s, a2a_r, x_s, x_r, y_s, y_r, fx_s, fx_r, fy_s, fy_r,
+    br_s, br_r, agf_s, agb_s, agz_r, agc_s, agc_r, pair_s, pair_r,
+    cf_s, cb_s, cf_r, cb_r, fin_s, fin_r,
+):
+    n_a = own_w_ref.shape[0]
+    n_tp = 2
+    z, y, x, c = [lax.axis_index(a) for a in AX]
+    place = (z * 2 + y) * 2 + x
+    places = n_a * 4
+    row_count, width = stream_ref.shape
+    half = row_count // n_tp
+    piece = own_w_ref.shape[1]
+    share = piece // 3
+    part = piece // 2
+    hi = z // 2
+    w = z + hi * (3 - 2 * z)
+    z_fwd = z + 1 - 2 * hi
+    z_back = z - 1 + 2 * hi
+    here = (z, y, x, c)
+    partner = (z, y, x, 1 - c)
+    x_next = (z, y, 1 - x, c)
+    y_next = (z, 1 - y, x, c)
+    fwd = (z_fwd, y, x, c)
+    back = (z_back, y, x, c)
+
+    def block_at(b):
+        return b + hi * (3 - 2 * b)
+
+    def remote(src, dst, s_sem, r_sem, device):
+        return pltpu.make_async_remote_copy(
+            src_ref=src, dst_ref=dst, send_sem=s_sem, recv_sem=r_sem,
+            device_id=device, device_id_type=MESH,
+        )
+
+    def at_place(p):
+        return (p // 4, (p // 2) % 2, p % 2, c)
+
+    head_cols = pl.ds(pl.multiple_of(c * HD, HD), HD)
+    edge = row_count - WIN
+    blocks = row_count // WIN
+
+    def halo_copies(to_next):
+        if to_next:
+            dev, src, dst, d_src, d_dst, o = at_place(place + 1), edge, 0, blocks - 1, 0, 0
+        else:
+            dev, src, dst, d_src, d_dst, o = at_place(place - 1), 0, row_count + WIN, 0, blocks + 1, 3
+        return [
+            remote(key_ref.at[pl.ds(src, WIN), head_cols], keys.at[pl.ds(dst, WIN)], halo_s.at[o], halo_r.at[o], dev),
+            remote(value_ref.at[pl.ds(src, WIN), head_cols], values.at[pl.ds(dst, WIN)], halo_s.at[o + 1], halo_r.at[o + 1], dev),
+            remote(docs_ref.at[d_src], docs.at[d_dst], halo_s.at[o + 2], halo_r.at[o + 2], dev),
+        ]
+
+    @pl.when(place < places - 1)
+    def _():
+        for cp in halo_copies(True):
+            cp.start()
+
+    @pl.when(place > 0)
+    def _():
+        for cp in halo_copies(False):
+            cp.start()
+
+    def column(zz, yy, xx):
+        return pl.ds(pl.multiple_of(((zz * 2 + yy) * 2 + xx) * HD, HD), HD)
+
+    peers = [z + 1 - 2 * (z % 2), (z + 2) % n_a, n_a - 1 - z]
+
+    def a2a(k):
+        to = peers[k]
+        return remote(own_w_ref.at[to], weights.at[:, column(z, y, x)], a2a_s.at[to], a2a_r.at[z], (to, y, x, c))
+
+    def a2a_arrived(k):
+        frm = peers[k]
+        remote(own_w_ref.at[frm], weights.at[:, column(frm, y, x)], a2a_s.at[frm], a2a_r.at[frm], here).wait_recv()
+
+    def side(zz, along_x):
+        block = weights.at[:, column(zz, y, x)]
+        if along_x:
+            return remote(block, block, x_s.at[zz], x_r.at[zz], x_next)
+        return remote(block, block, y_s.at[zz], y_r.at[zz], y_next)
+
+    def side_arrived(zz, along_x):
+        if along_x:
+            block = weights.at[:, column(zz, y, 1 - x)]
+            remote(block, block, x_s.at[zz], x_r.at[zz], here).wait_recv()
+        else:
+            block = weights.at[:, column(zz, 1 - y, x)]
+            remote(block, block, y_s.at[zz], y_r.at[zz], here).wait_recv()
+
+    def corner(zz, along_x):
+        if along_x:
+            block = weights.at[pl.ds(part, part), column(zz, 1 - y, x)]
+            return remote(block, block, fx_s.at[zz], fx_r.at[zz], x_next)
+        block = weights.at[pl.ds(0, part), column(zz, y, 1 - x)]
+        return remote(block, block, fy_s.at[zz], fy_r.at[zz], y_next)
+
+    def corner_arrived(zz, along_x):
+        first = part if along_x else 0
+        block = weights.at[pl.ds(first, part), column(zz, 1 - y, 1 - x)]
+        if along_x:
+            remote(block, block, fx_s.at[zz], fx_r.at[zz], here).wait_recv()
+        else:
+            remote(block, block, fy_s.at[zz], fy_r.at[zz], here).wait_recv()
+
+    own_first = [own_w_ref.at[z], weights.at[:, column(z, y, x)]]
+    start_x = remote(own_first[0], own_first[1], x_s.at[z], x_r.at[z], x_next)
+    start_y = remote(own_first[0], own_first[1], y_s.at[z], y_r.at[z], y_next)
+    for k in range(n_a - 1):
+        a2a(k).start()
+    start_x.start()
+    start_y.start()
+
+    keys[pl.ds(WIN, row_count), :] = key_ref[:, head_cols]
+    values[pl.ds(WIN, row_count), :] = value_ref[:, head_cols]
+    docs[pl.ds(1, blocks)] = docs_ref[...]
+
+    @pl.when(place == 0)
+    def _():
+        keys[pl.ds(0, WIN), :] = jnp.zeros((WIN, HD), keys.dtype)
+        values[pl.ds(0, WIN), :] = jnp.zeros((WIN, HD), values.dtype)
+        docs[0] = jnp.full((1, WIN), -1, jnp.int32)
+
+    @pl.when(place == places - 1)
+    def _():
+        keys[pl.ds(row_count + WIN, WIN), :] = jnp.zeros((WIN, HD), keys.dtype)
+        values[pl.ds(row_count + WIN, WIN), :] = jnp.zeros((WIN, HD), values.dtype)
+        docs[blocks + 1] = jnp.full((1, WIN), -1, jnp.int32)
+
+    heads_here = query_ref.shape[1] // HD
+    row_id = lax.broadcasted_iota(jnp.int32, (WIN, 3 * WIN), 0)
+    col_id = lax.broadcasted_iota(jnp.int32, (WIN, 3 * WIN), 1)
+    band = (col_id >= row_id) & (col_id <= row_id + 2 * WIN)
+
+    def attend(b):
+        mine = jnp.broadcast_to(docs[b + 1], (WIN, WIN)).T
+        key_docs = jnp.concatenate([jnp.broadcast_to(docs[b + t], (WIN, WIN)) for t in range(3)], axis=1)
+        query_docs = jnp.concatenate([mine] * 3, axis=1)
+        allowed = band & (key_docs == query_docs)
+        k_block = keys[pl.ds(b * WIN, 3 * WIN), :]
+        v_block = values[pl.ds(b * WIN, 3 * WIN), :]
+        for h in range(heads_here):
+            q = query_ref[pl.ds(b * WIN, WIN), pl.ds(h * HD, HD)]
+            scores = lax.dot_general(
+                q, k_block, (((1,), (1,)), ((), ())), preferred_element_type=jnp.float32
+            ) * HD ** (-0.5)
+            masked = jnp.where(allowed, scores, masked_low)
+            sink = sink_ref[h]
+            peak = jnp.maximum(jnp.max(masked, axis=1, keepdims=True), sink)
+            lifted = jnp.where(allowed, jnp.exp(masked - peak), 0.0)
+            denom = jnp.sum(lifted, axis=1, keepdims=True) + jnp.exp(sink - peak)
+            probs = (lifted / denom).astype(jnp.bfloat16)
+            got = jnp.dot(probs, v_block, preferred_element_type=jnp.float32)
+            attended[pl.ds(b * WIN, WIN), pl.ds(h * HD, HD)] = got.astype(jnp.bfloat16)
+
+    for b in range(1, blocks - 1):
+        attend(b)
+
+    @pl.when(place > 0)
+    def _():
+        for cp in halo_copies(True):
+            cp.wait_recv()
+
+    @pl.when(place < places - 1)
+    def _():
+        for cp in halo_copies(False):
+            cp.wait_recv()
+
+    attend(0)
+    attend(blocks - 1)
+
+    mine_rows = pl.ds(pl.multiple_of(c * half, half), half)
+    other_rows = pl.ds(pl.multiple_of((1 - c) * half, half), half)
+    branch_out[...] = jnp.dot(
+        attended[other_rows, :], out_w_ref[...], preferred_element_type=jnp.float32
+    ).astype(jnp.bfloat16)
+    branch_copy = remote(branch_out, branch_in, br_s, br_r, partner)
+    branch_copy.start()
+    weights[:, column(z, y, x)] = own_w_ref[z]
+    own_branch = jnp.dot(
+        attended[mine_rows, :], out_w_ref[...], preferred_element_type=jnp.float32
+    ).astype(jnp.bfloat16)
+    branch_copy.wait_recv()
+    branch = (own_branch.astype(jnp.float32) + branch_in[...].astype(jnp.float32)).astype(jnp.bfloat16)
+    carried = (
+        stream_ref[mine_rows, :].astype(jnp.float32) + branch.astype(jnp.float32)
+    ).astype(jnp.bfloat16)
+    carried_keep[...] = carried
+    carried_f = carried.astype(jnp.float32)
+    normed = (
+        carried_f
+        * lax.rsqrt(jnp.mean(carried_f * carried_f, axis=1, keepdims=True) + norm_eps)
+        * gain_ref[...]
+    ).astype(jnp.bfloat16)
+    rows[z, mine_rows, :] = normed
+
+    def ag(blk, to):
+        block = rows.at[blk, mine_rows]
+        if to == "core":
+            return remote(block, block, agc_s.at[blk], agc_r.at[blk], partner)
+        if to == "fwd":
+            return remote(block, block, agf_s.at[blk], agz_r.at[blk], fwd)
+        return remote(block, block, agb_s.at[blk], agz_r.at[blk], back)
+
+    def ag_arrived(blk):
+        block = rows.at[blk, mine_rows]
+        remote(block, block, agf_s.at[blk], agz_r.at[blk], here).wait_recv()
+
+    def ag_core_arrived(blk):
+        block = rows.at[blk, other_rows]
+        remote(block, block, agc_s.at[blk], agc_r.at[blk], here).wait_recv()
+
+    ag(z, "fwd").start()
+
+    @pl.when(w == 1)
+    def _():
+        ag(z, "back").start()
+
+    ag(z, "core").start()
+
+    def relay_rows(b_end, b_mid, mid_to):
+        @pl.when(w == 0)
+        def _():
+            ag_arrived(block_at(b_end))
+            ag(block_at(b_end), "core").start()
+
+        @pl.when(w == 1)
+        def _():
+            ag_arrived(block_at(b_mid))
+            ag(block_at(b_mid), mid_to).start()
+            ag(block_at(b_mid), "core").start()
+
+    def relay_corner(zz):
+        side_arrived(zz, True)
+        corner(zz, False).start()
+        side_arrived(zz, False)
+        corner(zz, True).start()
+
+    def relay_side(k):
+        a2a_arrived(k)
+        side(peers[k], True).start()
+        side(peers[k], False).start()
+
+    relay_side(0)
+    relay_corner(z)
+    relay_side(1)
+    relay_corner(peers[0])
+    relay_rows(1, 0, "fwd")
+    relay_side(2)
+    relay_corner(peers[1])
+    relay_rows(2, 2, "back")
+    relay_corner(peers[2])
+    for zz in [z] + peers:
+        corner_arrived(zz, True)
+        corner_arrived(zz, False)
+    relay_rows(3, 3, "back")
+
+    def blk_of(step):
+        order = [3 - 3 * hi, 2 - hi, 1 - z + 4 * hi, z]
+        if isinstance(step, int):
+            return order[step]
+        return jnp.where(step == 0, order[0], jnp.where(step == 1, order[1], jnp.where(step == 2, order[2], order[3])))
+
+    dims = (((1,), (1,)), ((), ()))
+
+    def pair(blk):
+        return remote(pair_out.at[blk], pair_in.at[blk], pair_s.at[blk], pair_r.at[blk], partner)
+
+    def chain_fwd_copy(step):
+        return remote(chain_out.at[step], chain_fwd.at[step], cf_s.at[step], cf_r.at[step], fwd)
+
+    def chain_mid_copy(step):
+        return remote(chain_out.at[step], chain_back.at[step], cf_s.at[step], cb_r.at[step], fwd)
+
+    chain_last = remote(chain_out.at[2], chain_back.at[0], cb_s, cb_r.at[0], back)
+
+    def feed_forward(step, _):
+        blk = blk_of(step)
+        ag_core_arrived(blk)
+        x_rows = rows[blk]
+        gate_acc = lax.dot_general(x_rows, weights[pl.ds(0, share), :], dims, preferred_element_type=jnp.float32)
+        up_acc = lax.dot_general(x_rows, weights[pl.ds(share, share), :], dims, preferred_element_type=jnp.float32)
+        hidden = (gate_acc / (1.0 + jnp.exp(-gate_acc)) * up_acc).astype(jnp.bfloat16)
+        hidden_keep[...] = hidden
+        pair_out[blk] = jnp.dot(
+            hidden_keep[other_rows, :], weights[pl.ds(2 * share, share), :], preferred_element_type=jnp.float32
+        ).astype(jnp.bfloat16)
+        pair(blk).start()
+        sum_keep[blk] = jnp.dot(
+            hidden_keep[mine_rows, :], weights[pl.ds(2 * share, share), :], preferred_element_type=jnp.float32
+        )
+
+        @pl.when((w == 0) & (step < 3))
+        def _():
+            pair(blk).wait_recv()
+            chain_out[step] = (sum_keep[blk] + pair_in[blk].astype(jnp.float32)).astype(jnp.bfloat16)
+            chain_fwd_copy(step).start()
+
+        return 0
+
+    lax.fori_loop(0, n_a, feed_forward, 0)
+
+    def chip_sum(blk):
+        return sum_keep[blk] + pair_in[blk].astype(jnp.float32)
+
+    def finish(total):
+        feed = total.astype(jnp.bfloat16).astype(jnp.float32)
+        mixed_ref[mine_rows, :] = (carried_keep[...].astype(jnp.float32) + 0.5 * feed).astype(jnp.bfloat16)
+
+    @pl.when(w == 0)
+    def _():
+        pair(z).wait_recv()
+        chain_last.wait_recv()
+        finish(chip_sum(z) + chain_back[0].astype(jnp.float32))
+
+    @pl.when(w == 1)
+    def _():
+        for step in range(2):
+            pair(blk_of(step)).wait_recv()
+            chain_fwd_copy(step).wait_recv()
+            chain_out[step] = (chip_sum(blk_of(step)) + chain_fwd[step].astype(jnp.float32)).astype(jnp.bfloat16)
+            chain_mid_copy(step).start()
+        pair(blk_of(2)).wait_recv()
+        chain_mid_copy(0).wait_recv()
+        chain_out[2] = (chip_sum(blk_of(2)) + chain_back[0].astype(jnp.float32)).astype(jnp.bfloat16)
+        chain_last.start()
+        pair(z).wait_recv()
+        chain_mid_copy(1).wait_recv()
+        chain_fwd_copy(2).wait_recv()
+        finish(chip_sum(z) + chain_fwd[2].astype(jnp.float32) + chain_back[1].astype(jnp.float32))
+
+    last = remote(mixed_ref.at[mine_rows], mixed_ref.at[mine_rows], fin_s, fin_r, partner)
+    last.start()
+
+    @pl.when(place < places - 1)
+    def _():
+        for cp in halo_copies(True):
+            cp.wait_send()
+
+    @pl.when(place > 0)
+    def _():
+        for cp in halo_copies(False):
+            cp.wait_send()
+
+    for k in range(n_a - 1):
+        a2a(k).wait_send()
+        side(peers[k], True).wait_send()
+        side(peers[k], False).wait_send()
+    start_x.wait_send()
+    start_y.wait_send()
+    for zz in [z] + peers:
+        corner(zz, True).wait_send()
+        corner(zz, False).wait_send()
+    branch_copy.wait_send()
+    for zz in [z] + peers:
+        ag(zz, "core").wait_send()
+        pair(zz).wait_send()
+    ag(z, "fwd").wait_send()
+
+    @pl.when(w == 0)
+    def _():
+        for step in range(3):
+            chain_fwd_copy(step).wait_send()
+
+    @pl.when(w == 1)
+    def _():
+        ag(z, "back").wait_send()
+        ag(block_at(0), "fwd").wait_send()
+        ag(block_at(2), "back").wait_send()
+        ag(block_at(3), "back").wait_send()
+        for step in range(2):
+            chain_mid_copy(step).wait_send()
+        chain_last.wait_send()
+
+    last.wait_send()
+    remote(mixed_ref.at[other_rows], mixed_ref.at[other_rows], fin_s, fin_r, partner).wait_recv()
+
+
+def fused_device(
+    stream, query_rows, key_rows, value_rows, doc_ids, sink_logit,
+    out_weight, norm_gain, gate_weight, up_weight, down_weight,
+):
+    n_a = lax.axis_size("sa")
+    row_count, width = stream.shape
+    half = row_count // 2
+    hidden_here = gate_weight.shape[1]
+    share = hidden_here // n_a
+    depth = gate_weight.shape[0]
+    own_w = jnp.concatenate(
+        [m.reshape(n_a, share, depth) for m in (gate_weight.T, up_weight.T, down_weight)], axis=1
+    )
+    docs = doc_ids.reshape(row_count // WIN, 1, WIN)
+    bf = jnp.bfloat16
+    vm = pltpu.VMEM
+    dma = pltpu.SemaphoreType.DMA
+    wide = row_count + 2 * WIN
+    scratch = [
+        vm((wide, HD), bf), vm((wide, HD), bf), vm((row_count // WIN + 2, 1, WIN), jnp.int32),
+        vm((row_count, query_rows.shape[1]), bf), vm((half, width), bf), vm((half, width), bf),
+        vm((half, width), bf), vm((n_a, row_count, width), bf), vm((3 * share, width), bf),
+        vm((row_count, share), bf),
+        vm((n_a, half, width), jnp.float32), vm((n_a, half, width), bf), vm((n_a, half, width), bf),
+        vm((3, half, width), bf), vm((3, half, width), bf), vm((2, half, width), bf),
+        dma((6,)), dma((6,)),
+        dma((n_a,)), dma((n_a,)), dma((n_a,)), dma((n_a,)), dma((n_a,)), dma((n_a,)),
+        dma((n_a,)), dma((n_a,)), dma((n_a,)), dma((n_a,)),
+        dma, dma, dma((n_a,)), dma((n_a,)), dma((n_a,)), dma((n_a,)), dma((n_a,)), dma((n_a,)), dma((n_a,)),
+        dma((3,)), dma, dma((3,)), dma((2,)), dma, dma,
+    ]
+    inside = pl.BlockSpec(memory_space=vm)
+    return pl.pallas_call(
+        fused,
+        out_shape=jax.ShapeDtypeStruct((row_count, width), bf),
+        in_specs=[inside] * 5 + [pl.BlockSpec(memory_space=pltpu.SMEM)] + [inside] * 3,
+        out_specs=inside,
+        scratch_shapes=scratch,
+        compiler_params=pltpu.CompilerParams(has_side_effects=True, vmem_limit_bytes=67043328),
+        name="fused_layer",
+    )(stream, query_rows, key_rows, value_rows, docs, sink_logit, out_weight, norm_gain.reshape(1, width), own_w)
+
+
 def solution(mesh):
     n_sp, n_tp = mesh.shape["sp"], mesh.shape["tp"]
     n_a = 4 if n_sp % 4 == 0 else 1
-    fine = Mesh(mesh.devices.reshape(n_a, n_sp // n_a, n_tp), ("sa", "sb", "tp"))
+    n_b = n_sp // n_a
+    if n_a == 4 and n_b == 4 and n_tp == KVH:
+        fine = Mesh(mesh.devices.reshape(n_a, 2, 2, n_tp), AX)
+        sp, body = AX[:3], fused_device
+    else:
+        fine = Mesh(mesh.devices.reshape(n_a, n_b, n_tp), ("sa", "sb", "tp"))
+        sp, body = SP, per_device
     in_specs = (
-        P(SP, None),
-        P(SP, "tp"),
-        P(SP, None),
-        P(SP, None),
-        P(SP),
+        P(sp, None),
+        P(sp, "tp"),
+        P(sp, None),
+        P(sp, None),
+        P(sp),
         P("tp"),
         P("tp", None),
         P(),
-        P(SP, "tp"),
-        P(SP, "tp"),
-        P("tp", SP),
+        P(sp, "tp"),
+        P(sp, "tp"),
+        P("tp", sp),
     )
-    return jax.shard_map(
-        per_device, mesh=fine, in_specs=in_specs, out_specs=P(SP, None), check_vma=False
-    )
+    return jax.shard_map(body, mesh=fine, in_specs=in_specs, out_specs=P(sp, None), check_vma=False)

time: 362 us -> 186 us (0.51)
  waiting for transfers between devices: 253 us -> 0 us
  Pallas kernels: 0 us -> 177 us
  matrix products: 37.1 us -> 0 us
  local copies, waits for them, and re-layouts: 28.9 us -> 6.97 us
  starting transfers between devices: 16.1 us -> 0 us
  between operations: 15.4 us -> 0.02 us
  other arithmetic: 10.4 us -> 1.49 us
    pallas_call x0 -> x1, Pallas kernels: none -> 177 us  [fused_device(): pl.pallas_call(fused, out_shape=jax.ShapeDtypeStruct((row_count, width),...]
    all_gather x4 -> x0, waiting for transfers between devices: 122 us -> none  [the longest x1 66.1 us: per_device(): rows_all = lax.all_gather(normed, ('sa', 'tp'), axis=0, tiled=True)]
    reduce_scatter x2 -> x0, waiting for transfers between devices: 69.5 us -> none  [the longest x1 69.4 us: per_device(): lax.psum_scatter(terms.astype(jnp.bfloat16), ('sa', 'tp'), scatter_dimens...]
    ppermute x8 -> x0, waiting for transfers between devices: 61.7 us -> none  [the longest x6 56.5 us: exchange(): lax.ppermute(out, 'sa', [(i, (i + k) % peers) for i in range(peers)])]
    dot_general x5 -> x0, matrix products: 37.1 us -> none  [the longest x1 21.3 us: per_device(): lax.dot_general(hidden, down_all, (((1,), (1,)), ((), ())), preferred_ele...]
    ppermute x8 -> x0, starting transfers between devices: 15.5 us -> none  [the longest x6 9.32 us: exchange(): lax.ppermute(out, 'sa', [(i, (i + k) % peers) for i in range(peers)])]
    mul x3 -> x0, local copies, waits for them, and re-layouts: 8.13 us -> none  [per_device(): mixed = (carried_f + 0.5 * feed.astype(jnp.float32)).astype(jnp.bfloat16)]
    concatenate x1 -> x0, local copies, waits for them, and re-layouts: 7.4 us -> none  [exchange(): both = jnp.concatenate(ring + ring, axis=0)]
  transfers between devices with their start and end apart: 14 -> 0, of which waited for: 11 -> 0; matrix products, arithmetic and copies ran while one was open for 8% -> 0% of each run, Pallas kernels for 0% -> 0%
where the time goes in v1:
time: 186 us
  Pallas kernels  177 us (95%)
  local copies, waits for them, and re-layouts  6.97 us (4%)
    pallas_call x1, Pallas kernels, fused_device(): pl.pallas_call(fused, out_shape=jax.ShapeDtypeStruct((row_count, width),...  177 us

profile of v1, /device:TPU:0, one launch (start us, length us, event | category | flops | bytes accessed | tf_op | source)
XLA Modules:
  0.0 185.9 jit_solution(17021239832770304684)
XLA Ops:
  0.0 0.0 copy-start
  0.0 1.3 reshape.15.docs_ref
  1.3 1.5 copy.12
  2.8 1.5 copy.13
  4.2 0.0 copy-done
  4.3 1.5 pad_maximum_fusion.own_w_ref
  5.7 177.4 %fused_layer.1 = bf16[384,2048]{1,0:T(8,128)(2,1)} custom-call(bf16[384,2048]{1,0:T(8,128)(2,1)} %stream_ref.1, bf16[384,512]{1,0:T(8,128)(2,1)} %query_ref.1, bf16[384,256]{1,0:T(8,128)(2,1)} %key_ref.1, bf16[384,256]{1,0:T(8,128)(2,1)} %value_ref.1, s32[3,1,128]{2,1,0:T(1,128)} %reshape.15.docs_ref, f32[4]{0:T(128)} %sink_ref.1, ...), custom_call_target="tpu_custom_call" | custom-call | tf_op jit(solution)/shard_map/fused_layer/pallas_call | solution.py:556
  183.1 2.7 %copy.15 = bf16[384,2048]{1,0:T(8,128)(2,1)} copy(bf16[384,2048]{1,0:T(8,128)(2,1)} %fused_layer.1) | data formatting | bytes 3145728
Async XLA Ops:
  0.0 4.3 %copy-start = (bf16[2816,128]{1,0:T(8,128)(2,1)S(1)}, bf16[2816,128]{1,0:T(8,128)(2,1)}, u32[]{:S(2)}) copy-start(bf16[2816,128]{1,0:T(8,128)(2,1)} %param.21) | copy-start | bytes 2162692

commit v2 on v0

--- a/solution.py
+++ b/solution.py
@@ -1,6 +1,8 @@
 import jax
 import jax.numpy as jnp
 from jax import lax
+from jax.experimental import pallas as pl
+from jax.experimental.pallas import tpu as pltpu
 from jax.sharding import Mesh, PartitionSpec as P
 
 HEADS = 8
@@ -133,23 +135,661 @@
     return lax.all_gather(mixed, "tp", axis=0, tiled=True)
 
 
+MESH = pl.DeviceIdType.MESH
+AX = ("sa", "sy", "sx", "tp")
+CHUNKS = 4
+UNITS = 2
+
+
+def fused(
+    stream_hbm, query_hbm, key_hbm, value_hbm, docs_ref, sink_ref, out_w_hbm, gain_ref,
+    gate_hbm, up_hbm, down_hbm,
+    mixed_ref,
+    stream_ref, query_ref, key_ref, value_ref, out_w_ref, gate_ref, up_ref, gate_t, up_t,
+    keys, values, docs, attended, branch_out, branch_in, carried_keep, rows, weights,
+    sum_keep, pair_out, pair_in, chain_out, chain_fwd, chain_back,
+    load_s, halo_s, halo_r, a2a_s, a2a_r, x_s, x_r, y_s, y_r, fx_s, fx_r, fy_s, fy_r,
+    br_s, br_r, agf_s, agb_s, agz_r, agc_s, agc_r, pair_s, pair_r,
+    cf_s, cl_s, cf_r, cb_r, fin_s, fin_r,
+):
+    n_a, row_count, width = rows.shape
+    n_tp = 2
+    z, y, x, c = [lax.axis_index(a) for a in AX]
+    place = (z * 2 + y) * 2 + x
+    places = n_a * 4
+    half = row_count // n_tp
+    size = half // CHUNKS
+    piece = weights.shape[0]
+    share = piece // 3
+    part = piece // 2
+    depth = gate_hbm.shape[0]
+    hi = z // 2
+    w = z + hi * (3 - 2 * z)
+    here = (z, y, x, c)
+    partner = (z, y, x, 1 - c)
+    x_next = (z, y, 1 - x, c)
+    y_next = (z, 1 - y, x, c)
+    fwd = (z + 1 - 2 * hi, y, x, c)
+    back = (z - 1 + 2 * hi, y, x, c)
+    peers = [z + 1 - 2 * (z % 2), (z + 2) % n_a, n_a - 1 - z]
+
+    def block_at(b):
+        return b + hi * (3 - 2 * b)
+
+    def remote(src, dst, s_sem, r_sem, device):
+        return pltpu.make_async_remote_copy(
+            src_ref=src, dst_ref=dst, send_sem=s_sem, recv_sem=r_sem,
+            device_id=device, device_id_type=MESH,
+        )
+
+    def at_place(p):
+        return (p // 4, (p // 2) % 2, p % 2, c)
+
+    head_cols = pl.ds(pl.multiple_of(c * HD, HD), HD)
+    edge = row_count - WIN
+    blocks = row_count // WIN
+
+    loads = [
+        pltpu.make_async_copy(a, b, load_s.at[i])
+        for i, (a, b) in enumerate([
+            (key_hbm.at[:, head_cols], key_ref), (value_hbm.at[:, head_cols], value_ref),
+            (gate_hbm, gate_ref), (up_hbm, up_ref), (query_hbm, query_ref),
+            (out_w_hbm, out_w_ref), (stream_hbm, stream_ref),
+        ])
+    ]
+    for cp in loads:
+        cp.start()
+
+    barrier = pltpu.get_barrier_semaphore()
+    nearby = [at_place((place + 1) % places), at_place((place + places - 1) % places)]
+    for device in [partner, x_next, y_next] + [(p, y, x, c) for p in peers] + nearby:
+        pl.semaphore_signal(barrier, inc=1, device_id=device, device_id_type=MESH)
+    pl.semaphore_wait(barrier, 8)
+    loads[0].wait()
+    loads[1].wait()
+
+    def halo_copies(to_next):
+        if to_next:
+            dev, src, dst, o = at_place(place + 1), edge, 0, 0
+        else:
+            dev, src, dst, o = at_place(place - 1), 0, row_count + WIN, 3
+        src, dst = pl.ds(src, WIN), pl.ds(dst, WIN)
+        return [
+            remote(key_ref.at[src], keys.at[dst], halo_s.at[o], halo_r.at[o], dev),
+            remote(value_ref.at[src], values.at[dst], halo_s.at[o + 1], halo_r.at[o + 1], dev),
+            remote(docs_ref.at[:, src], docs.at[:, dst], halo_s.at[o + 2], halo_r.at[o + 2], dev),
+        ]
+
+    @pl.when(place < places - 1)
+    def _():
+        for cp in halo_copies(True):
+            cp.start()
+
+    @pl.when(place > 0)
+    def _():
+        for cp in halo_copies(False):
+            cp.start()
+
+    def column(zz, yy, xx):
+        return pl.ds(pl.multiple_of(((zz * 2 + yy) * 2 + xx) * depth, depth), depth)
+
+    mine_col = column(z, y, x)
+
+    def own_piece(q, part_id, s_sem, r_sem, device):
+        src = (gate_t, up_t, down_hbm)[part_id].at[pl.ds(pl.multiple_of(q * share, 16), share)]
+        dst = weights.at[pl.ds(part_id * share, share), mine_col]
+        return remote(src, dst, s_sem, r_sem, device)
+
+    def a2a(k, part_id):
+        to = peers[k]
+        return own_piece(to, part_id, a2a_s.at[to], a2a_r.at[z], (to, y, x, c))
+
+    def own_x(part_id):
+        return own_piece(z, part_id, x_s.at[z], x_r.at[z], x_next)
+
+    def own_y(part_id):
+        return own_piece(z, part_id, y_s.at[z], y_r.at[z], y_next)
+
+    def wait_bytes(block, s_sem, r_sem):
+        return remote(block, block, s_sem, r_sem, here)
+
+    def side(zz, along_x):
+        block = weights.at[:, column(zz, y, x)]
+        if along_x:
+            return remote(block, block, x_s.at[zz], x_r.at[zz], x_next)
+        return remote(block, block, y_s.at[zz], y_r.at[zz], y_next)
+
+    def side_arrived(zz, along_x):
+        if along_x:
+            wait_bytes(weights.at[:, column(zz, y, 1 - x)], x_s.at[zz], x_r.at[zz]).wait_recv()
+        else:
+            wait_bytes(weights.at[:, column(zz, 1 - y, x)], y_s.at[zz], y_r.at[zz]).wait_recv()
+
+    def corner(zz, along_x):
+        if along_x:
+            block = weights.at[pl.ds(part, part), column(zz, 1 - y, x)]
+            return remote(block, block, fx_s.at[zz], fx_r.at[zz], x_next)
+        block = weights.at[pl.ds(0, part), column(zz, y, 1 - x)]
+        return remote(block, block, fy_s.at[zz], fy_r.at[zz], y_next)
+
+    def corner_arrived(zz):
+        wait_bytes(weights.at[pl.ds(part, part), column(zz, 1 - y, 1 - x)], fx_s.at[zz], fx_r.at[zz]).wait_recv()
+        wait_bytes(weights.at[pl.ds(0, part), column(zz, 1 - y, 1 - x)], fy_s.at[zz], fy_r.at[zz]).wait_recv()
+
+    a2a(0, 2).start()
+    own_x(2).start()
+    own_y(2).start()
+
+    @pl.when(w == 1)
+    def _():
+        a2a(2, 2).start()
+
+    own_down = pltpu.make_async_copy(
+        down_hbm.at[pl.ds(pl.multiple_of(z * share, 16), share)], weights.at[pl.ds(2 * share, share), mine_col], load_s.at[7]
+    )
+    own_down.start()
+
+    with jax.named_scope("turn"):
+        loads[2].wait()
+        loads[3].wait()
+
+        def turn(i, _):
+            at = pl.ds(pl.multiple_of(i * HD, HD), HD)
+            gate_t[at, :] = gate_ref[:, at].T
+            up_t[at, :] = up_ref[:, at].T
+            return 0
+
+        lax.fori_loop(0, gate_hbm.shape[1] // HD, turn, 0)
+
+    for part_id in range(2):
+        a2a(0, part_id).start()
+    for part_id in range(2):
+        own_x(part_id).start()
+        own_y(part_id).start()
+
+    @pl.when(w == 0)
+    def _():
+        a2a(2, 2).start()
+
+    for part_id in range(2):
+        a2a(2, part_id).start()
+
+    def far_send(k):
+        for part_id in range(3):
+            a2a(k, part_id).start()
+
+    @pl.when(w == 1)
+    def _():
+        far_send(1)
+
+    own_rows_w = pl.ds(pl.multiple_of(z * share, 16), share)
+    weights[pl.ds(0, share), mine_col] = gate_t[own_rows_w, :]
+    weights[pl.ds(share, share), mine_col] = up_t[own_rows_w, :]
+
+    keys[pl.ds(WIN, row_count), :] = key_ref[...]
+    values[pl.ds(WIN, row_count), :] = value_ref[...]
+    docs[:, pl.ds(WIN, row_count)] = docs_ref[...]
+
+    @pl.when(place == 0)
+    def _():
+        keys[pl.ds(0, WIN), :] = jnp.zeros((WIN, HD), keys.dtype)
+        values[pl.ds(0, WIN), :] = jnp.zeros((WIN, HD), values.dtype)
+        docs[:, pl.ds(0, WIN)] = jnp.full((1, WIN), -1, jnp.int32)
+
+    @pl.when(place == places - 1)
+    def _():
+        keys[pl.ds(row_count + WIN, WIN), :] = jnp.zeros((WIN, HD), keys.dtype)
+        values[pl.ds(row_count + WIN, WIN), :] = jnp.zeros((WIN, HD), values.dtype)
+        docs[:, pl.ds(row_count + WIN, WIN)] = jnp.full((1, WIN), -1, jnp.int32)
+
+    heads_here = query_ref.shape[1] // HD
+    row_id = lax.broadcasted_iota(jnp.int32, (WIN, 3 * WIN), 0)
+    col_id = lax.broadcasted_iota(jnp.int32, (WIN, 3 * WIN), 1)
+    band = (col_id >= row_id) & (col_id <= row_id + 2 * WIN)
+    loads[4].wait()
+
+    def attend(b):
+        mine = jnp.broadcast_to(docs[:, pl.ds((b + 1) * WIN, WIN)], (WIN, WIN)).T
+        key_docs = jnp.broadcast_to(docs[:, pl.ds(b * WIN, 3 * WIN)], (WIN, 3 * WIN))
+        query_docs = jnp.concatenate([mine] * 3, axis=1)
+        allowed = band & (key_docs == query_docs)
+        k_block = keys[pl.ds(b * WIN, 3 * WIN), :]
+        v_block = values[pl.ds(b * WIN, 3 * WIN), :]
+        for h in range(heads_here):
+            q = query_ref[pl.ds(b * WIN, WIN), pl.ds(h * HD, HD)]
+            scores = lax.dot_general(
+                q, k_block, (((1,), (1,)), ((), ())), preferred_element_type=jnp.float32
+            ) * HD ** (-0.5)
+            masked = jnp.where(allowed, scores, masked_low)
+            sink = sink_ref[h]
+            peak = jnp.maximum(jnp.max(masked, axis=1, keepdims=True), sink)
+            lifted = jnp.where(allowed, jnp.exp(masked - peak), 0.0)
+            denom = jnp.sum(lifted, axis=1, keepdims=True) + jnp.exp(sink - peak)
+            probs = (lifted / denom).astype(jnp.bfloat16)
+            got = jnp.dot(probs, v_block, preferred_element_type=jnp.float32)
+            attended[pl.ds(b * WIN, WIN), pl.ds(h * HD, HD)] = got.astype(jnp.bfloat16)
+
+    with jax.named_scope("attend_mid"):
+        for b in range(1, blocks - 1):
+            attend(b)
+
+    with jax.named_scope("halo_wait"):
+
+        @pl.when(place > 0)
+        def _():
+            for cp in halo_copies(True):
+                cp.wait_recv()
+
+        @pl.when(place < places - 1)
+        def _():
+            for cp in halo_copies(False):
+                cp.wait_recv()
+
+    with jax.named_scope("attend_edge"):
+        attend(0)
+        attend(blocks - 1)
+
+    mine_rows = pl.ds(pl.multiple_of(c * half, half), half)
+    other_rows = pl.ds(pl.multiple_of((1 - c) * half, half), half)
+    loads[5].wait()
+    loads[6].wait()
+    branch_out[...] = jnp.dot(
+        attended[other_rows, :], out_w_ref[...], preferred_element_type=jnp.float32
+    ).astype(jnp.bfloat16)
+    branch_copy = remote(branch_out, branch_in, br_s, br_r, partner)
+    branch_copy.start()
+    own_branch = jnp.dot(
+        attended[mine_rows, :], out_w_ref[...], preferred_element_type=jnp.float32
+    ).astype(jnp.bfloat16)
+    own_down.wait()
+    with jax.named_scope("branch_wait"):
+        branch_copy.wait_recv()
+    branch = (own_branch.astype(jnp.float32) + branch_in[...].astype(jnp.float32)).astype(jnp.bfloat16)
+    carried = (
+        stream_ref[mine_rows, :].astype(jnp.float32) + branch.astype(jnp.float32)
+    ).astype(jnp.bfloat16)
+    carried_keep[...] = carried
+    carried_f = carried.astype(jnp.float32)
+    normed = (
+        carried_f
+        * lax.rsqrt(jnp.mean(carried_f * carried_f, axis=1, keepdims=True) + norm_eps)
+        * gain_ref[...]
+    ).astype(jnp.bfloat16)
+    rows[z, mine_rows, :] = normed
+
+    def chunk_rows(core, j):
+        return pl.ds(pl.multiple_of(core * half + j * size, 16), size)
+
+    def ag(blk, j, to):
+        block = rows.at[blk, chunk_rows(c, j)]
+        if to == "core":
+            return remote(block, block, agc_s.at[blk, j], agc_r.at[blk, j], partner)
+        if to == "fwd":
+            return remote(block, block, agf_s.at[blk, j], agz_r.at[blk, j], fwd)
+        return remote(block, block, agb_s.at[blk, j], agz_r.at[blk, j], back)
+
+    def ag_arrived(blk, j):
+        wait_bytes(rows.at[blk, chunk_rows(c, j)], agf_s.at[blk, j], agz_r.at[blk, j]).wait_recv()
+
+    def ag_core_arrived(blk, j):
+        wait_bytes(rows.at[blk, chunk_rows(1 - c, j)], agc_s.at[blk, j], agc_r.at[blk, j]).wait_recv()
+
+    for j in range(CHUNKS):
+        ag(z, j, "fwd").start()
+
+    for j in range(CHUNKS):
+        ag(z, j, "core").start()
+
+    def far_sent(k):
+        wait_bytes(weights.at[:, mine_col], a2a_s.at[peers[k]], a2a_r.at[peers[k]]).wait_send()
+
+    def rows_back():
+        far_sent(1)
+        for j in range(CHUNKS):
+            ag(z, j, "back").start()
+
+    def relay_rows(b, j, to=None):
+        blk = block_at(b)
+        ag_arrived(blk, j)
+        if to is not None:
+            ag(blk, j, to).start()
+        ag(blk, j, "core").start()
+
+    def relay_corner(zz):
+        side_arrived(zz, True)
+        corner(zz, False).start()
+        side_arrived(zz, False)
+        corner(zz, True).start()
+
+    def relay_side(k):
+        frm = peers[k]
+        wait_bytes(weights.at[:, column(frm, y, x)], a2a_s.at[frm], a2a_r.at[frm]).wait_recv()
+        side(frm, True).start()
+        side(frm, False).start()
+
+    def run(plan):
+        for name, step, args in plan:
+            with jax.named_scope(name):
+                step(*args)
+
+    every = range(CHUNKS)
+
+    @pl.when(w == 0)
+    def _():
+        run(
+            [
+                ("side0", relay_side, (0,)),
+                ("corner_own", relay_corner, (z,)),
+                ("corner0", relay_corner, (peers[0],)),
+                ("side2", relay_side, (2,)),
+                ("side1", relay_side, (1,)),
+                ("far", far_send, (1,)),
+                ("corner2", relay_corner, (peers[2],)),
+            ]
+            + [("rows1", relay_rows, (1, j)) for j in every]
+            + [
+                ("corner1", relay_corner, (peers[1],)),
+                ("last_own", corner_arrived, (z,)),
+                ("last0", corner_arrived, (peers[0],)),
+                ("last2", corner_arrived, (peers[2],)),
+                ("last1", corner_arrived, (peers[1],)),
+            ]
+            + [("rows2", relay_rows, (2, j)) for j in every]
+        )
+
+    @pl.when(w == 1)
+    def _():
+        first, second = every[: CHUNKS // 2], every[CHUNKS // 2 :]
+        early = [[("rows0", relay_rows, (0, j, "fwd")), ("rows2", relay_rows, (2, j, "back"))] for j in first]
+        later = [[("rows0", relay_rows, (0, j, "fwd")), ("rows2", relay_rows, (2, j, "back"))] for j in second]
+        run(
+            [
+                ("side0", relay_side, (0,)),
+                ("corner_own", relay_corner, (z,)),
+                ("side2", relay_side, (2,)),
+                ("corner0", relay_corner, (peers[0],)),
+                ("rows_back", rows_back, ()),
+                ("corner2", relay_corner, (peers[2],)),
+                ("side1", relay_side, (1,)),
+            ]
+            + sum(early, [])
+            + [("corner1", relay_corner, (peers[1],))]
+            + sum(later, [])
+            + [
+                ("last_own", corner_arrived, (z,)),
+                ("last0", corner_arrived, (peers[0],)),
+                ("last2", corner_arrived, (peers[2],)),
+                ("last1", corner_arrived, (peers[1],)),
+            ]
+        )
+
+    def blk_of(step):
+        b = [2, 0, 1, 3]
+        if isinstance(step, int):
+            return block_at(b[step])
+        return jnp.where(
+            step == 0, block_at(b[0]),
+            jnp.where(step == 1, block_at(b[1]), jnp.where(step == 2, block_at(b[2]), block_at(b[3]))),
+        )
+
+    chain_b = [2, 3, 1]
+    dims = (((1,), (1,)), ((), ()))
+    unit = half // UNITS
+    per_unit = CHUNKS // UNITS
+
+    def unit_rows(u):
+        return pl.ds(pl.multiple_of(u * unit, 16), unit)
+
+    def pair(blk, u):
+        return remote(
+            pair_out.at[blk, unit_rows(u)], pair_in.at[blk, unit_rows(u)], pair_s.at[blk, u], pair_r.at[blk, u], partner
+        )
+
+    def chunk(j):
+        return pl.ds(pl.multiple_of(j * size, 16), size)
+
+    def chip_sum(blk, j):
+        return sum_keep[blk, chunk(j)] + pair_in[blk, chunk(j)].astype(jnp.float32)
+
+    def chain_fwd_copy(slot, j):
+        return remote(chain_out.at[slot, chunk(j)], chain_fwd.at[slot, chunk(j)], cf_s.at[slot, j], cf_r.at[slot, j], fwd)
+
+    def chain_mid_copy(slot, j):
+        return remote(chain_out.at[slot, chunk(j)], chain_back.at[1 - slot, chunk(j)], cf_s.at[slot, j], cb_r.at[1 - slot, j], fwd)
+
+    def chain_last_copy(j):
+        return remote(chain_out.at[2, chunk(j)], chain_back.at[0, chunk(j)], cl_s.at[j], cb_r.at[0, j], back)
+
+    def back_arrived(slot, j):
+        wait_bytes(chain_back.at[slot, chunk(j)], cl_s.at[j], cb_r.at[slot, j]).wait_recv()
+
+    def send_end(slot, u):
+        blk = block_at(chain_b[slot])
+        pair(blk, u).wait_recv()
+        for t in range(per_unit):
+            j = u * per_unit + t
+            chain_out[slot, chunk(j)] = chip_sum(blk, j).astype(jnp.bfloat16)
+            chain_fwd_copy(slot, j).start()
+
+    def feed_forward(i, _):
+        step = i // UNITS
+        u = i % UNITS
+
+        @pl.when((w == 1) & (i < CHUNKS))
+        def _():
+            relay_rows(3, i, "back")
+
+        @pl.when((w == 0) & (step == n_a - 1))
+        def _():
+            for t in range(per_unit):
+                relay_rows(3, u * per_unit + t)
+
+        blk = blk_of(step)
+        for t in range(per_unit):
+            ag_core_arrived(blk, u * per_unit + t)
+        x_rows = jnp.concatenate(
+            [rows[blk, pl.ds(pl.multiple_of(h * half + u * unit, 16), unit)] for h in (1 - c, c)], axis=0
+        )
+        gate_acc = lax.dot_general(x_rows, weights[pl.ds(0, share), :], dims, preferred_element_type=jnp.float32)
+        up_acc = lax.dot_general(x_rows, weights[pl.ds(share, share), :], dims, preferred_element_type=jnp.float32)
+        hidden = (gate_acc / (1.0 + jnp.exp(-gate_acc)) * up_acc).astype(jnp.bfloat16)
+        out = jnp.dot(hidden, weights[pl.ds(2 * share, share), :], preferred_element_type=jnp.float32)
+        pair_out[blk, unit_rows(u)] = out[:unit].astype(jnp.bfloat16)
+        pair(blk, u).start()
+        sum_keep[blk, unit_rows(u)] = out[unit:]
+
+        @pl.when((w == 0) & (step == 0))
+        def _():
+            send_end(0, u)
+
+        @pl.when((w == 0) & (step == n_a - 1))
+        def _():
+            send_end(1, u)
+
+        return 0
+
+    with jax.named_scope("ffn"):
+        lax.fori_loop(0, n_a * UNITS, feed_forward, 0)
+
+    def last(core, j):
+        block = mixed_ref.at[chunk_rows(core, j)]
+        return remote(block, block, fin_s.at[j], fin_r.at[j], partner)
+
+    def finish(j, total):
+        feed = total.astype(jnp.bfloat16).astype(jnp.float32)
+        mixed_ref[chunk_rows(c, j), :] = (
+            carried_keep[chunk(j)].astype(jnp.float32) + 0.5 * feed
+        ).astype(jnp.bfloat16)
+        last(c, j).start()
+
+    @pl.when(w == 0)
+    def _():
+        for u in range(UNITS):
+            send_end(2, u)
+        for u in range(UNITS):
+            pair(z, u).wait_recv()
+        for j in range(CHUNKS):
+            with jax.named_scope(f"fin{j}"):
+                back_arrived(0, j)
+                finish(j, chip_sum(z, j) + chain_back[0, chunk(j)].astype(jnp.float32))
+
+    @pl.when(w == 1)
+    def _():
+        for b in range(n_a):
+            for u in range(UNITS):
+                pair(block_at(b), u).wait_recv()
+
+        def pass_on(slot, j):
+            chain_fwd_copy(slot, j).wait_recv()
+            total = chip_sum(block_at(chain_b[slot]), j) + chain_fwd[slot, chunk(j)].astype(jnp.float32)
+            chain_out[slot, chunk(j)] = total.astype(jnp.bfloat16)
+            chain_mid_copy(slot, j).start()
+
+        def pass_back(j):
+            back_arrived(0, j)
+            total = chip_sum(block_at(0), j) + chain_back[0, chunk(j)].astype(jnp.float32)
+            chain_out[2, chunk(j)] = total.astype(jnp.bfloat16)
+            chain_last_copy(j).start()
+
+        def close(j):
+            back_arrived(1, j)
+            chain_fwd_copy(2, j).wait_recv()
+            finish(
+                j,
+                chip_sum(z, j)
+                + chain_fwd[2, chunk(j)].astype(jnp.float32)
+                + chain_back[1, chunk(j)].astype(jnp.float32),
+            )
+
+        plan = [("on0", pass_on, (0, j)) for j in range(CHUNKS)]
+        plan += [("on1", pass_on, (1, 0))]
+        for j in range(1, CHUNKS):
+            plan += [("on1", pass_on, (1, j)), ("pback", pass_back, (j - 1,))]
+        plan += [("pback", pass_back, (CHUNKS - 1,))]
+        plan += [("close", close, (j,)) for j in range(CHUNKS)]
+        run(plan)
+
+    with jax.named_scope("sends_done"):
+        @pl.when(place < places - 1)
+        def _():
+            for cp in halo_copies(True):
+                cp.wait_send()
+
+        @pl.when(place > 0)
+        def _():
+            for cp in halo_copies(False):
+                cp.wait_send()
+
+        whole = weights.at[:, mine_col]
+        far_sent(0)
+        far_sent(2)
+
+        @pl.when(w == 0)
+        def _():
+            far_sent(1)
+
+        for zz in [z] + peers:
+            wait_bytes(whole, x_s.at[zz], x_r.at[zz]).wait_send()
+            wait_bytes(whole, y_s.at[zz], y_r.at[zz]).wait_send()
+            corner(zz, True).wait_send()
+            corner(zz, False).wait_send()
+            for u in range(UNITS):
+                pair(zz, u).wait_send()
+            for j in range(CHUNKS):
+                ag(zz, j, "core").wait_send()
+        branch_copy.wait_send()
+        for j in range(CHUNKS):
+            ag(z, j, "fwd").wait_send()
+
+        @pl.when(w == 0)
+        def _():
+            for slot in range(3):
+                for j in range(CHUNKS):
+                    chain_fwd_copy(slot, j).wait_send()
+
+        @pl.when(w == 1)
+        def _():
+            for j in range(CHUNKS):
+                ag(z, j, "back").wait_send()
+                ag(block_at(0), j, "fwd").wait_send()
+                ag(block_at(2), j, "back").wait_send()
+                ag(block_at(3), j, "back").wait_send()
+                for slot in range(2):
+                    chain_mid_copy(slot, j).wait_send()
+                chain_last_copy(j).wait_send()
+
+        for j in range(CHUNKS):
+            last(c, j).wait_send()
+            last(1 - c, j).wait_recv()
+
+
+def fused_device(
+    stream, query_rows, key_rows, value_rows, doc_ids, sink_logit,
+    out_weight, norm_gain, gate_weight, up_weight, down_weight,
+):
+    n_a = lax.axis_size("sa")
+    row_count, width = stream.shape
+    half = row_count // 2
+    depth, hidden_here = gate_weight.shape
+    share = hidden_here // n_a
+    bf = jnp.bfloat16
+    vm = pltpu.VMEM
+    dma = pltpu.SemaphoreType.DMA
+    wide = row_count + 2 * WIN
+    per_block = dma((n_a,))
+    per_chunk = dma((n_a, CHUNKS))
+    per_unit = dma((n_a, UNITS))
+    scratch = [
+        vm((row_count, width), bf), vm(query_rows.shape, bf), vm((row_count, HD), bf), vm((row_count, HD), bf),
+        vm(out_weight.shape, bf), vm(gate_weight.shape, bf), vm(gate_weight.shape, bf),
+        vm((hidden_here, depth), bf), vm((hidden_here, depth), bf),
+        vm((wide, HD), bf), vm((wide, HD), bf), vm((1, wide), jnp.int32),
+        vm(query_rows.shape, bf), vm((half, width), bf), vm((half, width), bf),
+        vm((half, width), bf), vm((n_a, row_count, width), bf), vm((3 * share, width), bf),
+        vm((n_a, half, width), jnp.float32), vm((n_a, half, width), bf), vm((n_a, half, width), bf),
+        vm((3, half, width), bf), vm((3, half, width), bf), vm((2, half, width), bf),
+        dma((8,)), dma((6,)), dma((6,)),
+        *([per_block] * 10),
+        dma, dma, per_chunk, per_chunk, per_chunk, per_chunk, per_chunk, per_unit, per_unit,
+        dma((3, CHUNKS)), dma((CHUNKS,)), dma((3, CHUNKS)), dma((2, CHUNKS)), dma((CHUNKS,)), dma((CHUNKS,)),
+    ]
+    inside = pl.BlockSpec(memory_space=vm)
+    anywhere = pl.BlockSpec(memory_space=pl.ANY)
+    return pl.pallas_call(
+        fused,
+        out_shape=jax.ShapeDtypeStruct((row_count, width), bf),
+        in_specs=[anywhere] * 4 + [inside, pl.BlockSpec(memory_space=pltpu.SMEM), anywhere, inside] + [anywhere] * 3,
+        out_specs=inside,
+        scratch_shapes=scratch,
+        compiler_params=pltpu.CompilerParams(collective_id=0, has_side_effects=True, vmem_limit_bytes=56 * 2**20),
+        name="fused_layer",
+    )(
+        stream, query_rows, key_rows, value_rows, doc_ids.reshape(1, row_count), sink_logit, out_weight,
+        norm_gain.reshape(1, width), gate_weight, up_weight, down_weight,
+    )
+
+
 def solution(mesh):
     n_sp, n_tp = mesh.shape["sp"], mesh.shape["tp"]
     n_a = 4 if n_sp % 4 == 0 else 1
-    fine = Mesh(mesh.devices.reshape(n_a, n_sp // n_a, n_tp), ("sa", "sb", "tp"))
+    n_b = n_sp // n_a
+    if n_a == 4 and n_b == 4 and n_tp == KVH:
+        fine = Mesh(mesh.devices.reshape(n_a, 2, 2, n_tp), AX)
+        sp, body = AX[:3], fused_device
+    else:
+        fine = Mesh(mesh.devices.reshape(n_a, n_b, n_tp), ("sa", "sb", "tp"))
+        sp, body = SP, per_device
     in_specs = (
-        P(SP, None),
-        P(SP, "tp"),
-        P(SP, None),
-        P(SP, None),
-        P(SP),
+        P(sp, None),
+        P(sp, "tp"),
+        P(sp, None),
+        P(sp, None),
+        P(sp),
         P("tp"),
         P("tp", None),
         P(),
-        P(SP, "tp"),
-        P(SP, "tp"),
-        P("tp", SP),
+        P(sp, "tp"),
+        P(sp, "tp"),
+        P("tp", sp),
     )
-    return jax.shard_map(
-        per_device, mesh=fine, in_specs=in_specs, out_specs=P(SP, None), check_vma=False
-    )
+    return jax.shard_map(body, mesh=fine, in_specs=in_specs, out_specs=P(sp, None), check_vma=False)

time: 362 us -> 153 us (0.42)
  waiting for transfers between devices: 253 us -> 0 us
  Pallas kernels: 0 us -> 149 us
  matrix products: 37.1 us -> 0 us
  local copies, waits for them, and re-layouts: 28.9 us -> 3.97 us
  starting transfers between devices: 16.1 us -> 0 us
  between operations: 15.4 us -> 0.01 us
  other arithmetic: 10.4 us -> 0 us
    pallas_call x0 -> x1, Pallas kernels: none -> 149 us  [fused_device(): pl.pallas_call(fused, out_shape=jax.ShapeDtypeStruct((row_count, width),...]
    all_gather x4 -> x0, waiting for transfers between devices: 122 us -> none  [the longest x1 66.1 us: per_device(): rows_all = lax.all_gather(normed, ('sa', 'tp'), axis=0, tiled=True)]
    reduce_scatter x2 -> x0, waiting for transfers between devices: 69.5 us -> none  [the longest x1 69.4 us: per_device(): lax.psum_scatter(terms.astype(jnp.bfloat16), ('sa', 'tp'), scatter_dimens...]
    ppermute x8 -> x0, waiting for transfers between devices: 61.7 us -> none  [the longest x6 56.5 us: exchange(): lax.ppermute(out, 'sa', [(i, (i + k) % peers) for i in range(peers)])]
    dot_general x5 -> x0, matrix products: 37.1 us -> none  [the longest x1 21.3 us: per_device(): lax.dot_general(hidden, down_all, (((1,), (1,)), ((), ())), preferred_ele...]
    ppermute x8 -> x0, starting transfers between devices: 15.5 us -> none  [the longest x6 9.32 us: exchange(): lax.ppermute(out, 'sa', [(i, (i + k) % peers) for i in range(peers)])]
    mul x3 -> x0, local copies, waits for them, and re-layouts: 8.13 us -> none  [per_device(): mixed = (carried_f + 0.5 * feed.astype(jnp.float32)).astype(jnp.bfloat16)]
    concatenate x1 -> x0, local copies, waits for them, and re-layouts: 7.4 us -> none  [exchange(): both = jnp.concatenate(ring + ring, axis=0)]
  transfers between devices with their start and end apart: 14 -> 0, of which waited for: 11 -> 0; matrix products, arithmetic and copies ran while one was open for 8% -> 0% of each run, Pallas kernels for 0% -> 0%
where the time goes in v2:
time: 153 us
  Pallas kernels  149 us (97%)
  local copies, waits for them, and re-layouts  3.97 us (3%)
    pallas_call x1, Pallas kernels, fused_device(): pl.pallas_call(fused, out_shape=jax.ShapeDtypeStruct((row_count, width),...  149 us

profile of v2, /device:TPU:0, one launch (start us, length us, event | category | flops | bytes accessed | tf_op | source)
XLA Modules:
  0.0 153.1 jit_solution(16345836690359017658)
XLA Ops:
  0.0 1.2 reshape.6.docs_ref
  1.2 149.1 %fused_layer.1 = bf16[384,2048]{1,0:T(8,128)(2,1)} custom-call(bf16[384,2048]{1,0:T(8,128)(2,1)} %stream_hbm.1, bf16[384,512]{1,0:T(8,128)(2,1)} %query_hbm.1, bf16[384,256]{1,0:T(8,128)(2,1)} %key_hbm.1, bf16[384,256]{1,0:T(8,128)(2,1)} %value_hbm.1, s32[1,384]{1,0:T(1,128)} %reshape.6.docs_ref, f32[4]{0:T(128)} %sink_ref.1, bf16[512,2048]{1,0:T(8,128)(2,1)} %out_w_hbm.1, ...), custom_call_target="tpu_custom_call" | custom-call | tf_op jit(solution)/shard_map/fused_layer/pallas_call | solution.py:758
  150.4 2.7 %copy.13 = bf16[384,2048]{1,0:T(8,128)(2,1)} copy(bf16[384,2048]{1,0:T(8,128)(2,1)} %fused_layer.1) | data formatting | bytes 3145728

commit v3 on v2

--- a/solution.py
+++ b/solution.py
@@ -217,7 +217,7 @@
         return [
             remote(key_ref.at[src], keys.at[dst], halo_s.at[o], halo_r.at[o], dev),
             remote(value_ref.at[src], values.at[dst], halo_s.at[o + 1], halo_r.at[o + 1], dev),
-            remote(docs_ref.at[:, src], docs.at[:, dst], halo_s.at[o + 2], halo_r.at[o + 2], dev),
+            remote(docs_ref.at[src], docs.at[dst], halo_s.at[o + 2], halo_r.at[o + 2], dev),
         ]
 
     @pl.when(place < places - 1)
@@ -303,44 +303,39 @@
 
     for part_id in range(2):
         a2a(0, part_id).start()
+
+    @pl.when(w == 1)
+    def _():
+        for part_id in range(2):
+            a2a(2, part_id).start()
+
     for part_id in range(2):
         own_x(part_id).start()
         own_y(part_id).start()
 
-    @pl.when(w == 0)
-    def _():
-        a2a(2, 2).start()
-
-    for part_id in range(2):
-        a2a(2, part_id).start()
-
     def far_send(k):
         for part_id in range(3):
             a2a(k, part_id).start()
 
-    @pl.when(w == 1)
-    def _():
-        far_send(1)
-
     own_rows_w = pl.ds(pl.multiple_of(z * share, 16), share)
     weights[pl.ds(0, share), mine_col] = gate_t[own_rows_w, :]
     weights[pl.ds(share, share), mine_col] = up_t[own_rows_w, :]
 
     keys[pl.ds(WIN, row_count), :] = key_ref[...]
     values[pl.ds(WIN, row_count), :] = value_ref[...]
-    docs[:, pl.ds(WIN, row_count)] = docs_ref[...]
+    docs[pl.ds(WIN, row_count)] = docs_ref[...]
 
     @pl.when(place == 0)
     def _():
         keys[pl.ds(0, WIN), :] = jnp.zeros((WIN, HD), keys.dtype)
         values[pl.ds(0, WIN), :] = jnp.zeros((WIN, HD), values.dtype)
-        docs[:, pl.ds(0, WIN)] = jnp.full((1, WIN), -1, jnp.int32)
+        docs[pl.ds(0, WIN)] = jnp.full((WIN,), -1, jnp.int32)
 
     @pl.when(place == places - 1)
     def _():
         keys[pl.ds(row_count + WIN, WIN), :] = jnp.zeros((WIN, HD), keys.dtype)
         values[pl.ds(row_count + WIN, WIN), :] = jnp.zeros((WIN, HD), values.dtype)
-        docs[:, pl.ds(row_count + WIN, WIN)] = jnp.full((1, WIN), -1, jnp.int32)
+        docs[pl.ds(row_count + WIN, WIN)] = jnp.full((WIN,), -1, jnp.int32)
 
     heads_here = query_ref.shape[1] // HD
     row_id = lax.broadcasted_iota(jnp.int32, (WIN, 3 * WIN), 0)
@@ -349,8 +344,8 @@
     loads[4].wait()
 
     def attend(b):
-        mine = jnp.broadcast_to(docs[:, pl.ds((b + 1) * WIN, WIN)], (WIN, WIN)).T
-        key_docs = jnp.broadcast_to(docs[:, pl.ds(b * WIN, 3 * WIN)], (WIN, 3 * WIN))
+        mine = jnp.broadcast_to(docs[pl.ds((b + 1) * WIN, WIN)].reshape(1, WIN), (WIN, WIN)).T
+        key_docs = jnp.broadcast_to(docs[pl.ds(b * WIN, 3 * WIN)].reshape(1, 3 * WIN), (WIN, 3 * WIN))
         query_docs = jnp.concatenate([mine] * 3, axis=1)
         allowed = band & (key_docs == query_docs)
         k_block = keys[pl.ds(b * WIN, 3 * WIN), :]
@@ -435,10 +430,11 @@
         wait_bytes(rows.at[blk, chunk_rows(1 - c, j)], agc_s.at[blk, j], agc_r.at[blk, j]).wait_recv()
 
     for j in range(CHUNKS):
-        ag(z, j, "fwd").start()
-
-    for j in range(CHUNKS):
         ag(z, j, "core").start()
+
+    def rows_fwd():
+        for j in range(CHUNKS):
+            ag(z, j, "fwd").start()
 
     def far_sent(k):
         wait_bytes(weights.at[:, mine_col], a2a_s.at[peers[k]], a2a_r.at[peers[k]]).wait_send()
@@ -479,6 +475,8 @@
         run(
             [
                 ("side0", relay_side, (0,)),
+                ("far", far_send, (2,)),
+                ("rows_fwd", rows_fwd, ()),
                 ("corner_own", relay_corner, (z,)),
                 ("corner0", relay_corner, (peers[0],)),
                 ("side2", relay_side, (2,)),
@@ -499,12 +497,12 @@
 
     @pl.when(w == 1)
     def _():
-        first, second = every[: CHUNKS // 2], every[CHUNKS // 2 :]
-        early = [[("rows0", relay_rows, (0, j, "fwd")), ("rows2", relay_rows, (2, j, "back"))] for j in first]
-        later = [[("rows0", relay_rows, (0, j, "fwd")), ("rows2", relay_rows, (2, j, "back"))] for j in second]
+        both = [[("rows0", relay_rows, (0, j, "fwd")), ("rows2", relay_rows, (2, j, "back"))] for j in every]
         run(
             [
                 ("side0", relay_side, (0,)),
+                ("far", far_send, (1,)),
+                ("rows_fwd", rows_fwd, ()),
                 ("corner_own", relay_corner, (z,)),
                 ("side2", relay_side, (2,)),
                 ("corner0", relay_corner, (peers[0],)),
@@ -512,10 +510,9 @@
                 ("corner2", relay_corner, (peers[2],)),
                 ("side1", relay_side, (1,)),
             ]
-            + sum(early, [])
-            + [("corner1", relay_corner, (peers[1],))]
-            + sum(later, [])
+            + sum(both, [])
             + [
+                ("corner1", relay_corner, (peers[1],)),
                 ("last_own", corner_arrived, (z,)),
                 ("last0", corner_arrived, (peers[0],)),
                 ("last2", corner_arrived, (peers[2],)),
@@ -524,13 +521,8 @@
         )
 
     def blk_of(step):
-        b = [2, 0, 1, 3]
-        if isinstance(step, int):
-            return block_at(b[step])
-        return jnp.where(
-            step == 0, block_at(b[0]),
-            jnp.where(step == 1, block_at(b[1]), jnp.where(step == 2, block_at(b[2]), block_at(b[3]))),
-        )
+        late = jnp.where(step == 2, block_at(3 - 2 * w), block_at(1 + 2 * w))
+        return jnp.where(step == 0, block_at(2), jnp.where(step == 1, block_at(0), late))
 
     chain_b = [2, 3, 1]
     dims = (((1,), (1,)), ((), ()))
@@ -571,15 +563,30 @@
             chain_out[slot, chunk(j)] = chip_sum(blk, j).astype(jnp.bfloat16)
             chain_fwd_copy(slot, j).start()
 
+    def pass_on(slot, j):
+        chain_fwd_copy(slot, j).wait_recv()
+        total = chip_sum(block_at(chain_b[slot]), j) + chain_fwd[slot, chunk(j)].astype(jnp.float32)
+        chain_out[slot, chunk(j)] = total.astype(jnp.bfloat16)
+        chain_mid_copy(slot, j).start()
+
     def feed_forward(i, _):
         step = i // UNITS
         u = i % UNITS
 
-        @pl.when((w == 1) & (i < CHUNKS))
-        def _():
-            relay_rows(3, i, "back")
-
-        @pl.when((w == 0) & (step == n_a - 1))
+        @pl.when((w == 1) & (i >= 1) & (i <= CHUNKS))
+        def _():
+            relay_rows(3, i - 1, "back")
+
+        @pl.when((w == 1) & (i > CHUNKS))
+        def _():
+            @pl.when(i == CHUNKS + 1)
+            def _():
+                for v in range(UNITS):
+                    pair(block_at(2), v).wait_recv()
+
+            pass_on(0, i - CHUNKS - 1)
+
+        @pl.when((w == 0) & (step == 2))
         def _():
             for t in range(per_unit):
                 relay_rows(3, u * per_unit + t)
@@ -602,9 +609,13 @@
         def _():
             send_end(0, u)
 
-        @pl.when((w == 0) & (step == n_a - 1))
+        @pl.when((w == 0) & (step == 2))
         def _():
             send_end(1, u)
+
+        @pl.when((w == 0) & (step == 3))
+        def _():
+            send_end(2, u)
 
         return 0
 
@@ -625,8 +636,6 @@
     @pl.when(w == 0)
     def _():
         for u in range(UNITS):
-            send_end(2, u)
-        for u in range(UNITS):
             pair(z, u).wait_recv()
         for j in range(CHUNKS):
             with jax.named_scope(f"fin{j}"):
@@ -635,15 +644,9 @@
 
     @pl.when(w == 1)
     def _():
-        for b in range(n_a):
+        for b in (3, 0, 1):
             for u in range(UNITS):
                 pair(block_at(b), u).wait_recv()
-
-        def pass_on(slot, j):
-            chain_fwd_copy(slot, j).wait_recv()
-            total = chip_sum(block_at(chain_b[slot]), j) + chain_fwd[slot, chunk(j)].astype(jnp.float32)
-            chain_out[slot, chunk(j)] = total.astype(jnp.bfloat16)
-            chain_mid_copy(slot, j).start()
 
         def pass_back(j):
             back_arrived(0, j)
@@ -661,7 +664,7 @@
                 + chain_back[1, chunk(j)].astype(jnp.float32),
             )
 
-        plan = [("on0", pass_on, (0, j)) for j in range(CHUNKS)]
+        plan = [("on0", pass_on, (0, j)) for j in range(n_a * UNITS - CHUNKS - 1, CHUNKS)]
         plan += [("on1", pass_on, (1, 0))]
         for j in range(1, CHUNKS):
             plan += [("on1", pass_on, (1, j)), ("pback", pass_back, (j - 1,))]
@@ -743,7 +746,7 @@
         vm((row_count, width), bf), vm(query_rows.shape, bf), vm((row_count, HD), bf), vm((row_count, HD), bf),
         vm(out_weight.shape, bf), vm(gate_weight.shape, bf), vm(gate_weight.shape, bf),
         vm((hidden_here, depth), bf), vm((hidden_here, depth), bf),
-        vm((wide, HD), bf), vm((wide, HD), bf), vm((1, wide), jnp.int32),
+        vm((wide, HD), bf), vm((wide, HD), bf), vm((wide,), jnp.int32),
         vm(query_rows.shape, bf), vm((half, width), bf), vm((half, width), bf),
         vm((half, width), bf), vm((n_a, row_count, width), bf), vm((3 * share, width), bf),
         vm((n_a, half, width), jnp.float32), vm((n_a, half, width), bf), vm((n_a, half, width), bf),
@@ -757,14 +760,14 @@
     anywhere = pl.BlockSpec(memory_space=pl.ANY)
     return pl.pallas_call(
         fused,
-        out_shape=jax.ShapeDtypeStruct((row_count, width), bf),
+        out_shape=vm((row_count, width), bf),
         in_specs=[anywhere] * 4 + [inside, pl.BlockSpec(memory_space=pltpu.SMEM), anywhere, inside] + [anywhere] * 3,
         out_specs=inside,
         scratch_shapes=scratch,
         compiler_params=pltpu.CompilerParams(collective_id=0, has_side_effects=True, vmem_limit_bytes=56 * 2**20),
         name="fused_layer",
     )(
-        stream, query_rows, key_rows, value_rows, doc_ids.reshape(1, row_count), sink_logit, out_weight,
+        stream, query_rows, key_rows, value_rows, doc_ids, sink_logit, out_weight,
         norm_gain.reshape(1, width), gate_weight, up_weight, down_weight,
     )
 

time: 153 us -> 140 us (0.915)
  Pallas kernels: 149 us -> 137 us
  local copies, waits for them, and re-layouts: 3.97 us -> 1.15 us
    pallas_call x1, Pallas kernels: 149 us -> 137 us  [fused_device(): pl.pallas_call(fused, out_shape=vm((row_count, width), bf), in_specs=[any...]
    unnamed x1, local copies, waits for them, and re-layouts: 2.73 us -> 1.15 us
where the time goes in v3:
time: 140 us; the launch traced here: 139 us
  Pallas kernels  137 us (98%)
    pallas_call x1, Pallas kernels, fused_device(): pl.pallas_call(fused, out_shape=vm((row_count, width), bf), in_specs=[any...  137 us

profile of v3, /device:TPU:0, one launch (start us, length us, event | category | flops | bytes accessed | tf_op | source)
XLA Modules:
  0.0 138.6 jit_solution(7958903169581620630)
XLA Ops:
  0.0 137.4 %fused_layer.1 = bf16[384,2048]{1,0:T(8,128)(2,1)S(1)} custom-call(bf16[384,2048]{1,0:T(8,128)(2,1)} %stream_hbm.1, bf16[384,512]{1,0:T(8,128)(2,1)} %query_hbm.1, bf16[384,256]{1,0:T(8,128)(2,1)} %key_hbm.1, bf16[384,256]{1,0:T(8,128)(2,1)} %value_hbm.1, s32[384]{0:T(512)} %docs_ref.1, f32[4]{0:T(128)} %sink_ref.1, bf16[512,2048]{1,0:T(8,128)(2,1)} %out_w_hbm.1, ...), custom_call_target="tpu_custom_call" | custom-call | tf_op jit(solution)/shard_map/fused_layer/pallas_call | solution.py:761
  137.5 1.1 copy.13

commit v4 on v3

--- a/solution.py
+++ b/solution.py
@@ -141,6 +141,11 @@
 UNITS = 2
 
 
+def kind_shares(share):
+    shift = share // 14 // 16 * 16
+    return share - shift, share + shift
+
+
 def fused(
     stream_hbm, query_hbm, key_hbm, value_hbm, docs_ref, sink_ref, out_w_hbm, gain_ref,
     gate_hbm, up_hbm, down_hbm,
@@ -159,9 +164,7 @@
     places = n_a * 4
     half = row_count // n_tp
     size = half // CHUNKS
-    piece = weights.shape[0]
-    share = piece // 3
-    part = piece // 2
+    shares = kind_shares(gate_hbm.shape[1] // n_a)
     depth = gate_hbm.shape[0]
     hi = z // 2
     w = z + hi * (3 - 2 * z)
@@ -235,59 +238,84 @@
 
     mine_col = column(z, y, x)
 
-    def own_piece(q, part_id, s_sem, r_sem, device):
-        src = (gate_t, up_t, down_hbm)[part_id].at[pl.ds(pl.multiple_of(q * share, 16), share)]
+    def by_kind(act):
+        for kind in (0, 1):
+
+            @pl.when(w == kind)
+            def _(kind=kind):
+                act(kind)
+
+    def peer_kind(kind, k):
+        return kind if k == 2 else 1 - kind
+
+    def first_unit(q):
+        inner = shares[0] + (q // 2) * (shares[1] - shares[0])
+        return pl.multiple_of((q // 2) * (shares[0] + shares[1]) + (q % 2) * inner, 16)
+
+    def own_piece(q, kind, part_id, s_sem, r_sem, device):
+        share = shares[kind]
+        src = (gate_t, up_t, down_hbm)[part_id].at[pl.ds(first_unit(q), share)]
         dst = weights.at[pl.ds(part_id * share, share), mine_col]
         return remote(src, dst, s_sem, r_sem, device)
 
-    def a2a(k, part_id):
+    def a2a(kind, k, part_id):
         to = peers[k]
-        return own_piece(to, part_id, a2a_s.at[to], a2a_r.at[z], (to, y, x, c))
-
-    def own_x(part_id):
-        return own_piece(z, part_id, x_s.at[z], x_r.at[z], x_next)
-
-    def own_y(part_id):
-        return own_piece(z, part_id, y_s.at[z], y_r.at[z], y_next)
+        return own_piece(to, peer_kind(kind, k), part_id, a2a_s.at[to], a2a_r.at[z], (to, y, x, c))
+
+    def own_x(kind, part_id):
+        return own_piece(z, kind, part_id, x_s.at[z], x_r.at[z], x_next)
+
+    def own_y(kind, part_id):
+        return own_piece(z, kind, part_id, y_s.at[z], y_r.at[z], y_next)
+
+    def whole(kind, col):
+        return weights.at[pl.ds(0, 3 * shares[kind]), col]
+
+    def parts(kind, second):
+        cut = 3 * shares[kind] // 32 * 16
+        return pl.ds(cut, 3 * shares[kind] - cut) if second else pl.ds(0, cut)
 
     def wait_bytes(block, s_sem, r_sem):
         return remote(block, block, s_sem, r_sem, here)
 
-    def side(zz, along_x):
-        block = weights.at[:, column(zz, y, x)]
+    def side(kind, zz, along_x):
+        block = whole(kind, column(zz, y, x))
         if along_x:
             return remote(block, block, x_s.at[zz], x_r.at[zz], x_next)
         return remote(block, block, y_s.at[zz], y_r.at[zz], y_next)
 
-    def side_arrived(zz, along_x):
+    def side_arrived(kind, zz, along_x):
         if along_x:
-            wait_bytes(weights.at[:, column(zz, y, 1 - x)], x_s.at[zz], x_r.at[zz]).wait_recv()
+            wait_bytes(whole(kind, column(zz, y, 1 - x)), x_s.at[zz], x_r.at[zz]).wait_recv()
         else:
-            wait_bytes(weights.at[:, column(zz, 1 - y, x)], y_s.at[zz], y_r.at[zz]).wait_recv()
-
-    def corner(zz, along_x):
+            wait_bytes(whole(kind, column(zz, 1 - y, x)), y_s.at[zz], y_r.at[zz]).wait_recv()
+
+    def corner(kind, zz, along_x):
         if along_x:
-            block = weights.at[pl.ds(part, part), column(zz, 1 - y, x)]
+            block = weights.at[parts(kind, True), column(zz, 1 - y, x)]
             return remote(block, block, fx_s.at[zz], fx_r.at[zz], x_next)
-        block = weights.at[pl.ds(0, part), column(zz, y, 1 - x)]
+        block = weights.at[parts(kind, False), column(zz, y, 1 - x)]
         return remote(block, block, fy_s.at[zz], fy_r.at[zz], y_next)
 
-    def corner_arrived(zz):
-        wait_bytes(weights.at[pl.ds(part, part), column(zz, 1 - y, 1 - x)], fx_s.at[zz], fx_r.at[zz]).wait_recv()
-        wait_bytes(weights.at[pl.ds(0, part), column(zz, 1 - y, 1 - x)], fy_s.at[zz], fy_r.at[zz]).wait_recv()
-
-    a2a(0, 2).start()
-    own_x(2).start()
-    own_y(2).start()
-
-    @pl.when(w == 1)
-    def _():
-        a2a(2, 2).start()
-
-    own_down = pltpu.make_async_copy(
-        down_hbm.at[pl.ds(pl.multiple_of(z * share, 16), share)], weights.at[pl.ds(2 * share, share), mine_col], load_s.at[7]
-    )
-    own_down.start()
+    def corner_arrived(kind, zz):
+        far_col = column(zz, 1 - y, 1 - x)
+        wait_bytes(weights.at[parts(kind, True), far_col], fx_s.at[zz], fx_r.at[zz]).wait_recv()
+        wait_bytes(weights.at[parts(kind, False), far_col], fy_s.at[zz], fy_r.at[zz]).wait_recv()
+
+    def own_down(kind):
+        share = shares[kind]
+        return pltpu.make_async_copy(
+            down_hbm.at[pl.ds(first_unit(z), share)], weights.at[pl.ds(2 * share, share), mine_col], load_s.at[7]
+        )
+
+    @by_kind
+    def _(kind):
+        a2a(kind, 0, 2).start()
+        own_x(kind, 2).start()
+        own_y(kind, 2).start()
+        if kind == 1:
+            a2a(kind, 2, 2).start()
+        own_down(kind).start()
 
     with jax.named_scope("turn"):
         loads[2].wait()
@@ -301,25 +329,23 @@
 
         lax.fori_loop(0, gate_hbm.shape[1] // HD, turn, 0)
 
-    for part_id in range(2):
-        a2a(0, part_id).start()
-
-    @pl.when(w == 1)
-    def _():
+    @by_kind
+    def _(kind):
         for part_id in range(2):
-            a2a(2, part_id).start()
-
-    for part_id in range(2):
-        own_x(part_id).start()
-        own_y(part_id).start()
-
-    def far_send(k):
+            a2a(kind, 0, part_id).start()
+        if kind == 1:
+            for part_id in range(2):
+                a2a(kind, 2, part_id).start()
+        for part_id in range(2):
+            own_x(kind, part_id).start()
+            own_y(kind, part_id).start()
+        share = shares[kind]
+        weights[pl.ds(0, share), mine_col] = gate_t[pl.ds(first_unit(z), share), :]
+        weights[pl.ds(share, share), mine_col] = up_t[pl.ds(first_unit(z), share), :]
+
+    def far_send(kind, k):
         for part_id in range(3):
-            a2a(k, part_id).start()
-
-    own_rows_w = pl.ds(pl.multiple_of(z * share, 16), share)
-    weights[pl.ds(0, share), mine_col] = gate_t[own_rows_w, :]
-    weights[pl.ds(share, share), mine_col] = up_t[own_rows_w, :]
+            a2a(kind, k, part_id).start()
 
     keys[pl.ds(WIN, row_count), :] = key_ref[...]
     values[pl.ds(WIN, row_count), :] = value_ref[...]
@@ -396,7 +422,11 @@
     own_branch = jnp.dot(
         attended[mine_rows, :], out_w_ref[...], preferred_element_type=jnp.float32
     ).astype(jnp.bfloat16)
-    own_down.wait()
+
+    @by_kind
+    def _(kind):
+        own_down(kind).wait()
+
     with jax.named_scope("branch_wait"):
         branch_copy.wait_recv()
     branch = (own_branch.astype(jnp.float32) + branch_in[...].astype(jnp.float32)).astype(jnp.bfloat16)
@@ -436,11 +466,12 @@
         for j in range(CHUNKS):
             ag(z, j, "fwd").start()
 
-    def far_sent(k):
-        wait_bytes(weights.at[:, mine_col], a2a_s.at[peers[k]], a2a_r.at[peers[k]]).wait_send()
+    def far_sent(kind, k):
+        block = whole(peer_kind(kind, k), mine_col)
+        wait_bytes(block, a2a_s.at[peers[k]], a2a_r.at[peers[k]]).wait_send()
 
     def rows_back():
-        far_sent(1)
+        far_sent(1, 1)
         for j in range(CHUNKS):
             ag(z, j, "back").start()
 
@@ -451,17 +482,17 @@
             ag(blk, j, to).start()
         ag(blk, j, "core").start()
 
-    def relay_corner(zz):
-        side_arrived(zz, True)
-        corner(zz, False).start()
-        side_arrived(zz, False)
-        corner(zz, True).start()
-
-    def relay_side(k):
+    def relay_corner(kind, zz):
+        side_arrived(kind, zz, True)
+        corner(kind, zz, False).start()
+        side_arrived(kind, zz, False)
+        corner(kind, zz, True).start()
+
+    def relay_side(kind, k):
         frm = peers[k]
-        wait_bytes(weights.at[:, column(frm, y, x)], a2a_s.at[frm], a2a_r.at[frm]).wait_recv()
-        side(frm, True).start()
-        side(frm, False).start()
+        wait_bytes(whole(kind, column(frm, y, x)), a2a_s.at[frm], a2a_r.at[frm]).wait_recv()
+        side(kind, frm, True).start()
+        side(kind, frm, False).start()
 
     def run(plan):
         for name, step, args in plan:
@@ -469,65 +500,61 @@
                 step(*args)
 
     every = range(CHUNKS)
-
-    @pl.when(w == 0)
-    def _():
+    unit = half // UNITS
+    per_unit = CHUNKS // UNITS
+
+    def gather_end():
         run(
             [
-                ("side0", relay_side, (0,)),
-                ("far", far_send, (2,)),
+                ("corner_own", relay_corner, (0, z)),
+                ("side0", relay_side, (0, 0)),
+                ("far", far_send, (0, 2)),
                 ("rows_fwd", rows_fwd, ()),
-                ("corner_own", relay_corner, (z,)),
-                ("corner0", relay_corner, (peers[0],)),
-                ("side2", relay_side, (2,)),
-                ("side1", relay_side, (1,)),
-                ("far", far_send, (1,)),
-                ("corner2", relay_corner, (peers[2],)),
+                ("corner0", relay_corner, (0, peers[0])),
+                ("side2", relay_side, (0, 2)),
+                ("side1", relay_side, (0, 1)),
+                ("far", far_send, (0, 1)),
+                ("corner2", relay_corner, (0, peers[2])),
             ]
             + [("rows1", relay_rows, (1, j)) for j in every]
             + [
-                ("corner1", relay_corner, (peers[1],)),
-                ("last_own", corner_arrived, (z,)),
-                ("last0", corner_arrived, (peers[0],)),
-                ("last2", corner_arrived, (peers[2],)),
-                ("last1", corner_arrived, (peers[1],)),
+                ("corner1", relay_corner, (0, peers[1])),
+                ("last_own", corner_arrived, (0, z)),
+                ("last0", corner_arrived, (0, peers[0])),
+                ("last2", corner_arrived, (0, peers[2])),
             ]
-            + [("rows2", relay_rows, (2, j)) for j in every]
+            + [("rows2", relay_rows, (2, j)) for j in range(per_unit)]
+            + [("last1", corner_arrived, (0, peers[1]))]
         )
 
-    @pl.when(w == 1)
-    def _():
+    def gather_middle():
         both = [[("rows0", relay_rows, (0, j, "fwd")), ("rows2", relay_rows, (2, j, "back"))] for j in every]
         run(
             [
-                ("side0", relay_side, (0,)),
-                ("far", far_send, (1,)),
+                ("corner_own", relay_corner, (1, z)),
+                ("side0", relay_side, (1, 0)),
+                ("far", far_send, (1, 1)),
                 ("rows_fwd", rows_fwd, ()),
-                ("corner_own", relay_corner, (z,)),
-                ("side2", relay_side, (2,)),
-                ("corner0", relay_corner, (peers[0],)),
+                ("side2", relay_side, (1, 2)),
+                ("corner0", relay_corner, (1, peers[0])),
                 ("rows_back", rows_back, ()),
-                ("corner2", relay_corner, (peers[2],)),
-                ("side1", relay_side, (1,)),
+                ("corner2", relay_corner, (1, peers[2])),
+                ("side1", relay_side, (1, 1)),
             ]
             + sum(both, [])
             + [
-                ("corner1", relay_corner, (peers[1],)),
-                ("last_own", corner_arrived, (z,)),
-                ("last0", corner_arrived, (peers[0],)),
-                ("last2", corner_arrived, (peers[2],)),
-                ("last1", corner_arrived, (peers[1],)),
+                ("corner1", relay_corner, (1, peers[1])),
+                ("rows3", relay_rows, (3, 0, "back")),
+                ("last_own", corner_arrived, (1, z)),
+                ("last0", corner_arrived, (1, peers[0])),
+                ("last2", corner_arrived, (1, peers[2])),
+                ("rows3", relay_rows, (3, 1, "back")),
+                ("last1", corner_arrived, (1, peers[1])),
             ]
         )
 
-    def blk_of(step):
-        late = jnp.where(step == 2, block_at(3 - 2 * w), block_at(1 + 2 * w))
-        return jnp.where(step == 0, block_at(2), jnp.where(step == 1, block_at(0), late))
-
     chain_b = [2, 3, 1]
     dims = (((1,), (1,)), ((), ()))
-    unit = half // UNITS
-    per_unit = CHUNKS // UNITS
 
     def unit_rows(u):
         return pl.ds(pl.multiple_of(u * unit, 16), unit)
@@ -569,31 +596,10 @@
         chain_out[slot, chunk(j)] = total.astype(jnp.bfloat16)
         chain_mid_copy(slot, j).start()
 
-    def feed_forward(i, _):
-        step = i // UNITS
-        u = i % UNITS
-
-        @pl.when((w == 1) & (i >= 1) & (i <= CHUNKS))
-        def _():
-            relay_rows(3, i - 1, "back")
-
-        @pl.when((w == 1) & (i > CHUNKS))
-        def _():
-            @pl.when(i == CHUNKS + 1)
-            def _():
-                for v in range(UNITS):
-                    pair(block_at(2), v).wait_recv()
-
-            pass_on(0, i - CHUNKS - 1)
-
-        @pl.when((w == 0) & (step == 2))
-        def _():
-            for t in range(per_unit):
-                relay_rows(3, u * per_unit + t)
-
-        blk = blk_of(step)
+    def feed_forward(kind, blk, u):
         for t in range(per_unit):
             ag_core_arrived(blk, u * per_unit + t)
+        share = shares[kind]
         x_rows = jnp.concatenate(
             [rows[blk, pl.ds(pl.multiple_of(h * half + u * unit, 16), unit)] for h in (1 - c, c)], axis=0
         )
@@ -605,22 +611,68 @@
         pair(blk, u).start()
         sum_keep[blk, unit_rows(u)] = out[unit:]
 
-        @pl.when((w == 0) & (step == 0))
+    def pick(step, order):
+        late = jnp.where(step == 2, block_at(order[2]), block_at(order[3]))
+        return jnp.where(step == 0, block_at(order[0]), jnp.where(step == 1, block_at(order[1]), late))
+
+    def end_unit(i, _):
+        step, u = i // UNITS, i % UNITS
+
+        @pl.when(i == 1)
         def _():
-            send_end(0, u)
-
-        @pl.when((w == 0) & (step == 2))
+            for j in range(per_unit, CHUNKS):
+                relay_rows(2, j)
+
+        @pl.when(step == 2)
         def _():
-            send_end(1, u)
-
-        @pl.when((w == 0) & (step == 3))
-        def _():
-            send_end(2, u)
+            for t in range(per_unit):
+                relay_rows(3, u * per_unit + t)
+
+        feed_forward(0, pick(step, (2, 0, 3, 1)), u)
+        for at, slot in ((0, 0), (2, 1), (3, 2)):
+
+            @pl.when(step == at)
+            def _(slot=slot):
+                send_end(slot, u)
 
         return 0
 
-    with jax.named_scope("ffn"):
-        lax.fori_loop(0, n_a * UNITS, feed_forward, 0)
+    def middle_unit(i, _):
+        def back_rows(j):
+            relay_rows(3, j, "back")
+
+        def pair_come(b, v):
+            pair(block_at(b), v).wait_recv()
+
+        tasks = {
+            1: [(back_rows, 2), (pair_come, 2, 0), (pass_on, 0, 0)],
+            2: [(back_rows, 3), (pass_on, 0, 1)],
+            3: [(pair_come, 2, 1), (pass_on, 0, 2)],
+            4: [(pass_on, 0, 3)],
+            6: [(pair_come, 3, 0), (pass_on, 1, 0)],
+            7: [(pair_come, 3, 1), (pass_on, 1, 1)],
+        }
+        for at, todo in tasks.items():
+
+            @pl.when(i == at)
+            def _(todo=todo):
+                for act, *args in todo:
+                    act(*args)
+
+        feed_forward(1, pick(i // UNITS, (2, 3, 0, 1)), i % UNITS)
+        return 0
+
+    @pl.when(w == 0)
+    def _():
+        gather_end()
+        with jax.named_scope("ffn"):
+            lax.fori_loop(0, n_a * UNITS, end_unit, 0)
+
+    @pl.when(w == 1)
+    def _():
+        gather_middle()
+        with jax.named_scope("ffn"):
+            lax.fori_loop(0, n_a * UNITS, middle_unit, 0)
 
     def last(core, j):
         block = mixed_ref.at[chunk_rows(core, j)]
@@ -644,7 +696,7 @@
 
     @pl.when(w == 1)
     def _():
-        for b in (3, 0, 1):
+        for b in (0, 1):
             for u in range(UNITS):
                 pair(block_at(b), u).wait_recv()
 
@@ -664,10 +716,8 @@
                 + chain_back[1, chunk(j)].astype(jnp.float32),
             )
 
-        plan = [("on0", pass_on, (0, j)) for j in range(n_a * UNITS - CHUNKS - 1, CHUNKS)]
-        plan += [("on1", pass_on, (1, 0))]
-        for j in range(1, CHUNKS):
-            plan += [("on1", pass_on, (1, j)), ("pback", pass_back, (j - 1,))]
+        plan = [("on1", pass_on, (1, 2)), ("pback", pass_back, (0,)), ("on1", pass_on, (1, 3))]
+        plan += [("pback", pass_back, (1,)), ("pback", pass_back, (2,))]
         plan += [("pback", pass_back, (CHUNKS - 1,))]
         plan += [("close", close, (j,)) for j in range(CHUNKS)]
         run(plan)
@@ -683,19 +733,19 @@
             for cp in halo_copies(False):
                 cp.wait_send()
 
-        whole = weights.at[:, mine_col]
-        far_sent(0)
-        far_sent(2)
-
-        @pl.when(w == 0)
-        def _():
-            far_sent(1)
+        @by_kind
+        def _(kind):
+            far_sent(kind, 0)
+            far_sent(kind, 2)
+            if kind == 0:
+                far_sent(kind, 1)
+            for zz in [z] + peers:
+                wait_bytes(whole(kind, mine_col), x_s.at[zz], x_r.at[zz]).wait_send()
+                wait_bytes(whole(kind, mine_col), y_s.at[zz], y_r.at[zz]).wait_send()
+                corner(kind, zz, True).wait_send()
+                corner(kind, zz, False).wait_send()
 
         for zz in [z] + peers:
-            wait_bytes(whole, x_s.at[zz], x_r.at[zz]).wait_send()
-            wait_bytes(whole, y_s.at[zz], y_r.at[zz]).wait_send()
-            corner(zz, True).wait_send()
-            corner(zz, False).wait_send()
             for u in range(UNITS):
                 pair(zz, u).wait_send()
             for j in range(CHUNKS):
@@ -748,7 +798,7 @@
         vm((hidden_here, depth), bf), vm((hidden_here, depth), bf),
         vm((wide, HD), bf), vm((wide, HD), bf), vm((wide,), jnp.int32),
         vm(query_rows.shape, bf), vm((half, width), bf), vm((half, width), bf),
-        vm((half, width), bf), vm((n_a, row_count, width), bf), vm((3 * share, width), bf),
+        vm((half, width), bf), vm((n_a, row_count, width), bf), vm((3 * max(kind_shares(share)), width), bf),
         vm((n_a, half, width), jnp.float32), vm((n_a, half, width), bf), vm((n_a, half, width), bf),
         vm((3, half, width), bf), vm((3, half, width), bf), vm((2, half, width), bf),
         dma((8,)), dma((6,)), dma((6,)),

time: 140 us -> 137 us (0.979)
  Pallas kernels: 137 us -> 135 us
    pallas_call x1, Pallas kernels: 137 us -> 135 us  [fused_device(): pl.pallas_call(fused, out_shape=vm((row_count, width), bf), in_specs=[any...]
where the time goes in v4:
time: 137 us; the launch traced here: 136 us
  Pallas kernels  135 us (99%)
    pallas_call x1, Pallas kernels, fused_device(): pl.pallas_call(fused, out_shape=vm((row_count, width), bf), in_specs=[any...  135 us

profile of v4, /device:TPU:0, one launch (start us, length us, event | category | flops | bytes accessed | tf_op | source)
XLA Modules:
  0.0 135.8 jit_solution(10714409428739459081)
XLA Ops:
  0.0 134.7 %fused_layer.1 = bf16[384,2048]{1,0:T(8,128)(2,1)S(1)} custom-call(bf16[384,2048]{1,0:T(8,128)(2,1)} %stream_hbm.1, bf16[384,512]{1,0:T(8,128)(2,1)} %query_hbm.1, bf16[384,256]{1,0:T(8,128)(2,1)} %key_hbm.1, bf16[384,256]{1,0:T(8,128)(2,1)} %value_hbm.1, s32[384]{0:T(512)} %docs_ref.1, f32[4]{0:T(128)} %sink_ref.1, bf16[512,2048]{1,0:T(8,128)(2,1)} %out_w_hbm.1, ...), custom_call_target="tpu_custom_call" | custom-call | tf_op jit(solution)/shard_map/fused_layer/pallas_call | solution.py:811
  134.7 1.1 copy.13

commit v5 on v4

--- a/solution.py
+++ b/solution.py
@@ -200,13 +200,12 @@
             (out_w_hbm, out_w_ref), (stream_hbm, stream_ref),
         ])
     ]
-    for cp in loads:
-        cp.start()
-
     barrier = pltpu.get_barrier_semaphore()
     nearby = [at_place((place + 1) % places), at_place((place + places - 1) % places)]
     for device in [partner, x_next, y_next] + [(p, y, x, c) for p in peers] + nearby:
         pl.semaphore_signal(barrier, inc=1, device_id=device, device_id_type=MESH)
+    for cp in loads:
+        cp.start()
     pl.semaphore_wait(barrier, 8)
     loads[0].wait()
     loads[1].wait()
@@ -263,10 +262,10 @@
         return own_piece(to, peer_kind(kind, k), part_id, a2a_s.at[to], a2a_r.at[z], (to, y, x, c))
 
     def own_x(kind, part_id):
-        return own_piece(z, kind, part_id, x_s.at[z], x_r.at[z], x_next)
+        return own_piece(z, kind, part_id, x_s, x_r.at[z], x_next)
 
     def own_y(kind, part_id):
-        return own_piece(z, kind, part_id, y_s.at[z], y_r.at[z], y_next)
+        return own_piece(z, kind, part_id, y_s, y_r.at[z], y_next)
 
     def whole(kind, col):
         return weights.at[pl.ds(0, 3 * shares[kind]), col]
@@ -281,26 +280,26 @@
     def side(kind, zz, along_x):
         block = whole(kind, column(zz, y, x))
         if along_x:
-            return remote(block, block, x_s.at[zz], x_r.at[zz], x_next)
-        return remote(block, block, y_s.at[zz], y_r.at[zz], y_next)
+            return remote(block, block, x_s, x_r.at[zz], x_next)
+        return remote(block, block, y_s, y_r.at[zz], y_next)
 
     def side_arrived(kind, zz, along_x):
         if along_x:
-            wait_bytes(whole(kind, column(zz, y, 1 - x)), x_s.at[zz], x_r.at[zz]).wait_recv()
+            wait_bytes(whole(kind, column(zz, y, 1 - x)), x_s, x_r.at[zz]).wait_recv()
         else:
-            wait_bytes(whole(kind, column(zz, 1 - y, x)), y_s.at[zz], y_r.at[zz]).wait_recv()
+            wait_bytes(whole(kind, column(zz, 1 - y, x)), y_s, y_r.at[zz]).wait_recv()
 
     def corner(kind, zz, along_x):
         if along_x:
             block = weights.at[parts(kind, True), column(zz, 1 - y, x)]
-            return remote(block, block, fx_s.at[zz], fx_r.at[zz], x_next)
+            return remote(block, block, fx_s, fx_r.at[zz], x_next)
         block = weights.at[parts(kind, False), column(zz, y, 1 - x)]
-        return remote(block, block, fy_s.at[zz], fy_r.at[zz], y_next)
+        return remote(block, block, fy_s, fy_r.at[zz], y_next)
 
     def corner_arrived(kind, zz):
         far_col = column(zz, 1 - y, 1 - x)
-        wait_bytes(weights.at[parts(kind, True), far_col], fx_s.at[zz], fx_r.at[zz]).wait_recv()
-        wait_bytes(weights.at[parts(kind, False), far_col], fy_s.at[zz], fy_r.at[zz]).wait_recv()
+        wait_bytes(weights.at[parts(kind, True), far_col], fx_s, fx_r.at[zz]).wait_recv()
+        wait_bytes(weights.at[parts(kind, False), far_col], fy_s, fy_r.at[zz]).wait_recv()
 
     def own_down(kind):
         share = shares[kind]
@@ -448,16 +447,16 @@
     def ag(blk, j, to):
         block = rows.at[blk, chunk_rows(c, j)]
         if to == "core":
-            return remote(block, block, agc_s.at[blk, j], agc_r.at[blk, j], partner)
+            return remote(block, block, agc_s, agc_r.at[blk, j], partner)
         if to == "fwd":
-            return remote(block, block, agf_s.at[blk, j], agz_r.at[blk, j], fwd)
-        return remote(block, block, agb_s.at[blk, j], agz_r.at[blk, j], back)
+            return remote(block, block, agf_s, agz_r.at[blk, j], fwd)
+        return remote(block, block, agb_s, agz_r.at[blk, j], back)
 
     def ag_arrived(blk, j):
-        wait_bytes(rows.at[blk, chunk_rows(c, j)], agf_s.at[blk, j], agz_r.at[blk, j]).wait_recv()
+        wait_bytes(rows.at[blk, chunk_rows(c, j)], agf_s, agz_r.at[blk, j]).wait_recv()
 
     def ag_core_arrived(blk, j):
-        wait_bytes(rows.at[blk, chunk_rows(1 - c, j)], agc_s.at[blk, j], agc_r.at[blk, j]).wait_recv()
+        wait_bytes(rows.at[blk, chunk_rows(1 - c, j)], agc_s, agc_r.at[blk, j]).wait_recv()
 
     for j in range(CHUNKS):
         ag(z, j, "core").start()
@@ -510,8 +509,8 @@
                 ("side0", relay_side, (0, 0)),
                 ("far", far_send, (0, 2)),
                 ("rows_fwd", rows_fwd, ()),
+                ("side2", relay_side, (0, 2)),
                 ("corner0", relay_corner, (0, peers[0])),
-                ("side2", relay_side, (0, 2)),
                 ("side1", relay_side, (0, 1)),
                 ("far", far_send, (0, 1)),
                 ("corner2", relay_corner, (0, peers[2])),
@@ -561,7 +560,7 @@
 
     def pair(blk, u):
         return remote(
-            pair_out.at[blk, unit_rows(u)], pair_in.at[blk, unit_rows(u)], pair_s.at[blk, u], pair_r.at[blk, u], partner
+            pair_out.at[blk, unit_rows(u)], pair_in.at[blk, unit_rows(u)], pair_s, pair_r.at[blk, u], partner
         )
 
     def chunk(j):
@@ -571,16 +570,16 @@
         return sum_keep[blk, chunk(j)] + pair_in[blk, chunk(j)].astype(jnp.float32)
 
     def chain_fwd_copy(slot, j):
-        return remote(chain_out.at[slot, chunk(j)], chain_fwd.at[slot, chunk(j)], cf_s.at[slot, j], cf_r.at[slot, j], fwd)
+        return remote(chain_out.at[slot, chunk(j)], chain_fwd.at[slot, chunk(j)], cf_s, cf_r.at[slot, j], fwd)
 
     def chain_mid_copy(slot, j):
-        return remote(chain_out.at[slot, chunk(j)], chain_back.at[1 - slot, chunk(j)], cf_s.at[slot, j], cb_r.at[1 - slot, j], fwd)
+        return remote(chain_out.at[slot, chunk(j)], chain_back.at[1 - slot, chunk(j)], cf_s, cb_r.at[1 - slot, j], fwd)
 
     def chain_last_copy(j):
-        return remote(chain_out.at[2, chunk(j)], chain_back.at[0, chunk(j)], cl_s.at[j], cb_r.at[0, j], back)
+        return remote(chain_out.at[2, chunk(j)], chain_back.at[0, chunk(j)], cl_s, cb_r.at[0, j], back)
 
     def back_arrived(slot, j):
-        wait_bytes(chain_back.at[slot, chunk(j)], cl_s.at[j], cb_r.at[slot, j]).wait_recv()
+        wait_bytes(chain_back.at[slot, chunk(j)], cl_s, cb_r.at[slot, j]).wait_recv()
 
     def send_end(slot, u):
         blk = block_at(chain_b[slot])
@@ -676,7 +675,7 @@
 
     def last(core, j):
         block = mixed_ref.at[chunk_rows(core, j)]
-        return remote(block, block, fin_s.at[j], fin_r.at[j], partner)
+        return remote(block, block, fin_s, fin_r.at[j], partner)
 
     def finish(j, total):
         feed = total.astype(jnp.bfloat16).astype(jnp.float32)
@@ -739,41 +738,31 @@
             far_sent(kind, 2)
             if kind == 0:
                 far_sent(kind, 1)
-            for zz in [z] + peers:
-                wait_bytes(whole(kind, mine_col), x_s.at[zz], x_r.at[zz]).wait_send()
-                wait_bytes(whole(kind, mine_col), y_s.at[zz], y_r.at[zz]).wait_send()
-                corner(kind, zz, True).wait_send()
-                corner(kind, zz, False).wait_send()
-
-        for zz in [z] + peers:
-            for u in range(UNITS):
-                pair(zz, u).wait_send()
-            for j in range(CHUNKS):
-                ag(zz, j, "core").wait_send()
+            four = pl.ds(0, n_a * depth)
+            wait_bytes(whole(kind, four), x_s, x_r.at[0]).wait_send()
+            wait_bytes(whole(kind, four), y_s, y_r.at[0]).wait_send()
+            wait_bytes(weights.at[parts(kind, True), four], fx_s, fx_r.at[0]).wait_send()
+            wait_bytes(weights.at[parts(kind, False), four], fy_s, fy_r.at[0]).wait_send()
+
+        wait_bytes(pair_out, pair_s, pair_r.at[0, 0]).wait_send()
+        wait_bytes(rows.at[:, mine_rows], agc_s, agc_r.at[0, 0]).wait_send()
         branch_copy.wait_send()
-        for j in range(CHUNKS):
-            ag(z, j, "fwd").wait_send()
 
         @pl.when(w == 0)
         def _():
-            for slot in range(3):
-                for j in range(CHUNKS):
-                    chain_fwd_copy(slot, j).wait_send()
+            wait_bytes(rows.at[z, mine_rows], agf_s, agz_r.at[0, 0]).wait_send()
+            wait_bytes(chain_out, cf_s, cf_r.at[0, 0]).wait_send()
 
         @pl.when(w == 1)
         def _():
-            for j in range(CHUNKS):
-                ag(z, j, "back").wait_send()
-                ag(block_at(0), j, "fwd").wait_send()
-                ag(block_at(2), j, "back").wait_send()
-                ag(block_at(3), j, "back").wait_send()
-                for slot in range(2):
-                    chain_mid_copy(slot, j).wait_send()
-                chain_last_copy(j).wait_send()
+            wait_bytes(rows.at[pl.ds(0, 2), mine_rows], agf_s, agz_r.at[0, 0]).wait_send()
+            wait_bytes(rows.at[pl.ds(0, 3), mine_rows], agb_s, agz_r.at[0, 0]).wait_send()
+            wait_bytes(chain_out.at[pl.ds(0, 2)], cf_s, cf_r.at[0, 0]).wait_send()
+            wait_bytes(chain_out.at[2], cl_s, cb_r.at[0, 0]).wait_send()
 
         for j in range(CHUNKS):
-            last(c, j).wait_send()
             last(1 - c, j).wait_recv()
+        wait_bytes(mixed_ref.at[mine_rows], fin_s, fin_r.at[0]).wait_send()
 
 
 def fused_device(
@@ -801,10 +790,10 @@
         vm((half, width), bf), vm((n_a, row_count, width), bf), vm((3 * max(kind_shares(share)), width), bf),
         vm((n_a, half, width), jnp.float32), vm((n_a, half, width), bf), vm((n_a, half, width), bf),
         vm((3, half, width), bf), vm((3, half, width), bf), vm((2, half, width), bf),
-        dma((8,)), dma((6,)), dma((6,)),
-        *([per_block] * 10),
-        dma, dma, per_chunk, per_chunk, per_chunk, per_chunk, per_chunk, per_unit, per_unit,
-        dma((3, CHUNKS)), dma((CHUNKS,)), dma((3, CHUNKS)), dma((2, CHUNKS)), dma((CHUNKS,)), dma((CHUNKS,)),
+        dma((8,)), dma((6,)), dma((6,)), per_block, per_block,
+        *([dma, per_block] * 4),
+        dma, dma, dma, dma, per_chunk, dma, per_chunk, dma, per_unit,
+        dma, dma, dma((3, CHUNKS)), dma((2, CHUNKS)), dma, dma((CHUNKS,)),
     ]
     inside = pl.BlockSpec(memory_space=vm)
     anywhere = pl.BlockSpec(memory_space=pl.ANY)

time: 137 us -> 135 us (0.985)
  no operation moved by 1% of the time
where the time goes in v5:
time: 135 us
  Pallas kernels  134 us (99%)
    pallas_call x1, Pallas kernels, fused_device(): pl.pallas_call(fused, out_shape=vm((row_count, width), bf), in_specs=[any...  134 us

profile of v5, /device:TPU:0, one launch (start us, length us, event | category | flops | bytes accessed | tf_op | source)
XLA Modules:
  0.0 135.0 jit_solution(4957913938502192235)
XLA Ops:
  0.0 133.8 %fused_layer.1 = bf16[384,2048]{1,0:T(8,128)(2,1)S(1)} custom-call(bf16[384,2048]{1,0:T(8,128)(2,1)} %stream_hbm.1, bf16[384,512]{1,0:T(8,128)(2,1)} %query_hbm.1, bf16[384,256]{1,0:T(8,128)(2,1)} %key_hbm.1, bf16[384,256]{1,0:T(8,128)(2,1)} %value_hbm.1, s32[384]{0:T(512)} %docs_ref.1, f32[4]{0:T(128)} %sink_ref.1, bf16[512,2048]{1,0:T(8,128)(2,1)} %out_w_hbm.1, ...), custom_call_target="tpu_custom_call" | custom-call | tf_op jit(solution)/shard_map/fused_layer/pallas_call | solution.py:800
  133.8 1.1 copy.13

commit v6 on v5

--- a/solution.py
+++ b/solution.py
@@ -292,14 +292,14 @@
     def corner(kind, zz, along_x):
         if along_x:
             block = weights.at[parts(kind, True), column(zz, 1 - y, x)]
-            return remote(block, block, fx_s, fx_r.at[zz], x_next)
+            return remote(block, block, fx_s, fx_r, x_next)
         block = weights.at[parts(kind, False), column(zz, y, 1 - x)]
-        return remote(block, block, fy_s, fy_r.at[zz], y_next)
-
-    def corner_arrived(kind, zz):
-        far_col = column(zz, 1 - y, 1 - x)
-        wait_bytes(weights.at[parts(kind, True), far_col], fx_s, fx_r.at[zz]).wait_recv()
-        wait_bytes(weights.at[parts(kind, False), far_col], fy_s, fy_r.at[zz]).wait_recv()
+        return remote(block, block, fy_s, fy_r, y_next)
+
+    def corners_arrived(kind):
+        four = pl.ds(0, n_a * depth)
+        wait_bytes(weights.at[parts(kind, True), four], fx_s, fx_r).wait_recv()
+        wait_bytes(weights.at[parts(kind, False), four], fy_s, fy_r).wait_recv()
 
     def own_down(kind):
         share = shares[kind]
@@ -518,12 +518,9 @@
             + [("rows1", relay_rows, (1, j)) for j in every]
             + [
                 ("corner1", relay_corner, (0, peers[1])),
-                ("last_own", corner_arrived, (0, z)),
-                ("last0", corner_arrived, (0, peers[0])),
-                ("last2", corner_arrived, (0, peers[2])),
             ]
             + [("rows2", relay_rows, (2, j)) for j in range(per_unit)]
-            + [("last1", corner_arrived, (0, peers[1]))]
+            + [("last", corners_arrived, (0,))]
         )
 
     def gather_middle():
@@ -544,11 +541,8 @@
             + [
                 ("corner1", relay_corner, (1, peers[1])),
                 ("rows3", relay_rows, (3, 0, "back")),
-                ("last_own", corner_arrived, (1, z)),
-                ("last0", corner_arrived, (1, peers[0])),
-                ("last2", corner_arrived, (1, peers[2])),
                 ("rows3", relay_rows, (3, 1, "back")),
-                ("last1", corner_arrived, (1, peers[1])),
+                ("last", corners_arrived, (1,)),
             ]
         )
 
@@ -741,8 +735,8 @@
             four = pl.ds(0, n_a * depth)
             wait_bytes(whole(kind, four), x_s, x_r.at[0]).wait_send()
             wait_bytes(whole(kind, four), y_s, y_r.at[0]).wait_send()
-            wait_bytes(weights.at[parts(kind, True), four], fx_s, fx_r.at[0]).wait_send()
-            wait_bytes(weights.at[parts(kind, False), four], fy_s, fy_r.at[0]).wait_send()
+            wait_bytes(weights.at[parts(kind, True), four], fx_s, fx_r).wait_send()
+            wait_bytes(weights.at[parts(kind, False), four], fy_s, fy_r).wait_send()
 
         wait_bytes(pair_out, pair_s, pair_r.at[0, 0]).wait_send()
         wait_bytes(rows.at[:, mine_rows], agc_s, agc_r.at[0, 0]).wait_send()
@@ -791,7 +785,7 @@
         vm((n_a, half, width), jnp.float32), vm((n_a, half, width), bf), vm((n_a, half, width), bf),
         vm((3, half, width), bf), vm((3, half, width), bf), vm((2, half, width), bf),
         dma((8,)), dma((6,)), dma((6,)), per_block, per_block,
-        *([dma, per_block] * 4),
+        *([dma, per_block] * 2), *([dma] * 4),
         dma, dma, dma, dma, per_chunk, dma, per_chunk, dma, per_unit,
         dma, dma, dma((3, CHUNKS)), dma((2, CHUNKS)), dma, dma((CHUNKS,)),
     ]

time: 135 us -> 135 us (level)
  no operation moved by 1% of the time
where the time goes in v6:
time: 135 us
  Pallas kernels  134 us (99%)
    pallas_call x1, Pallas kernels, fused_device(): pl.pallas_call(fused, out_shape=vm((row_count, width), bf), in_specs=[any...  134 us

profile of v6, /device:TPU:0, one launch (start us, length us, event | category | flops | bytes accessed | tf_op | source)
XLA Modules:
  0.0 134.9 jit_solution(4162630709566639757)
XLA Ops:
  0.0 133.8 %fused_layer.1 = bf16[384,2048]{1,0:T(8,128)(2,1)S(1)} custom-call(bf16[384,2048]{1,0:T(8,128)(2,1)} %stream_hbm.1, bf16[384,512]{1,0:T(8,128)(2,1)} %query_hbm.1, bf16[384,256]{1,0:T(8,128)(2,1)} %key_hbm.1, bf16[384,256]{1,0:T(8,128)(2,1)} %value_hbm.1, s32[384]{0:T(512)} %docs_ref.1, f32[4]{0:T(128)} %sink_ref.1, bf16[512,2048]{1,0:T(8,128)(2,1)} %out_w_hbm.1, ...), custom_call_target="tpu_custom_call" | custom-call | tf_op jit(solution)/shard_map/fused_layer/pallas_call | solution.py:794
  133.8 1.1 copy.13
